TPU v7x, 32 devices: a whole 2x2x4 slice. The times are simulated.
32 devices in a mesh: sp: 8 (over z, y), dp: 4 (over x, core).
Axes of the slice: x: 2, y: 2, z: 4, core: 2. Of those that a mesh axis runs over, the one named last changes fastest.
Arguments:
- query_nope: bfloat16 [4, 2048, 16, 128], P('dp', 'sp'), may hold values from -6 to 6
- query_rope: bfloat16 [4, 2048, 16, 64], P('dp', 'sp'), may hold values from -160 to 160
- latent: bfloat16 [4, 2048, 256], P('dp', 'sp'), may hold values from -6 to 6
- key_rope: bfloat16 [4, 2048, 64], P('dp', 'sp'), may hold values from -4 to 4
- resid: bfloat16 [4, 2048, 2048], P('dp', 'sp'), may hold values from -6 to 6
- latent_gain: float32 [256], replicated, may hold values from 0.1 to 1.9
- key_up: bfloat16 [256, 2048], P(None, 'sp'), may hold values from -0.375 to 0.375
- value_up: bfloat16 [256, 2048], P(None, 'sp'), may hold values from -0.375 to 0.375
- out_proj: bfloat16 [2048, 2048], P('sp', 'dp'), may hold values from -0.125 to 0.125
- norm_gain: float32 [2048], replicated, may hold values from 0.1 to 1.9
- expert_gate: bfloat16 [8, 2048, 1024], P('sp'), may hold values from -0.125 to 0.125
- expert_up: bfloat16 [8, 2048, 1024], P('sp'), may hold values from -0.125 to 0.125
- expert_down: bfloat16 [8, 1024, 2048], P('sp'), may hold values from -0.1875 to 0.1875
- routes: int32 [4, 2048, 2], P('dp', 'sp'), may hold values from 0 to 7, all different within a row; in each aligned block of 256 rows (0 to 255, 256 to 511, ..., all dimensions but the last counted through in order) at most 128 rows name the same one
- route_weight: float32 [4, 2048, 2], P('dp', 'sp'), may hold values from 0.2 to 1
Outputs:
- mixed: bfloat16 [4, 2048, 2048], P('dp', 'sp')
Inputs may be any that keep to these rules, and one draw needn't show every extreme that they name: `routes`: each token names two different experts. Among the tokens of one device no expert is named more than 128 times, and in every draw some expert is named exactly 128 times by some device's tokens.
All inputs are finite; a program needn't handle non-finite values.
Results may differ from a plain program's by a relative error of at most 0.0075.
Values may be sent and summed in bfloat16 or wider, within the bound.
A program may use at most 128 MiB of HBM per device.

v0:
```python
import functools
import math

import jax
import jax.numpy as jnp
from jax import lax
from jax.experimental import pallas as pl
from jax.experimental.pallas import tpu as pltpu
from jax.sharding import PartitionSpec as P

epsilon = 1e-06
rope_base = 10000.0
masked_score = -1e30
log2_e = 1.4426950408889634


def rotate(values, positions):
    half_width = values.shape[-1] // 2
    frequency = rope_base ** (-jnp.arange(half_width, dtype=jnp.float32) / half_width)
    angles = positions.astype(jnp.float32)[:, None] * frequency[None, :]
    cosine = jnp.cos(angles)
    sine_part = jnp.sin(angles)
    if values.ndim == 3:
        cosine = cosine[:, None, :]
        sine_part = sine_part[:, None, :]
    floats = values.astype(jnp.float32)
    first_half = floats[..., :half_width]
    second_half = floats[..., half_width:]
    turned = jnp.concatenate(
        [
            first_half * cosine - second_half * sine_part,
            second_half * cosine + first_half * sine_part,
        ],
        axis=-1,
    )
    return turned.astype(jnp.bfloat16)


def rms_scaled(values, gain):
    floats = values.astype(jnp.float32)
    return floats * lax.rsqrt(jnp.mean(floats * floats, axis=-1, keepdims=True) + epsilon) * gain


def attend_kernel(heads_here, nope, channels, scale, me_ref, query_ref, shared_ref, ups_ref, out_ref):
    group = pl.program_id(0)
    columns = heads_here * nope
    me = me_ref[0]
    tokens = shared_ref.shape[1]
    ups = ups_ref[...].reshape(channels, 2 * columns)
    up_keys = ups[:, 0:columns]
    up_values = ups[:, columns : 2 * columns]
    up_values_t = jnp.transpose(up_values.astype(jnp.float32)).astype(jnp.bfloat16)

    def scores_of(chunk):
        latent = shared_ref[chunk, :, 0:channels]
        turned = shared_ref[chunk, :, channels:]
        keys = jnp.dot(latent, up_keys, preferred_element_type=jnp.float32).astype(jnp.bfloat16)
        values_t = lax.dot_general(
            up_values_t, latent, (((1,), (1,)), ((), ())), preferred_element_type=jnp.float32
        ).astype(jnp.bfloat16)
        scores = []
        for head in range(heads_here):
            full = jnp.concatenate([keys[:, head * nope : (head + 1) * nope], turned], axis=1)
            scores.append(
                jnp.dot(full, query_ref[head], preferred_element_type=jnp.float32)
                * (scale * log2_e)
            )
        return scores, [values_t[h * nope : (h + 1) * nope, :] for h in range(heads_here)]

    key_ids = lax.broadcasted_iota(jnp.int32, (tokens, tokens), 0)
    query_ids = lax.broadcasted_iota(jnp.int32, (tokens, tokens), 1)
    allowed = key_ids <= query_ids
    scores, values = scores_of(me)
    state = []
    for score, value in zip(scores, values):
        score = jnp.where(allowed, score, masked_score)
        largest = jnp.max(score, axis=0, keepdims=True)
        powers = jnp.exp2(score - largest)
        state.append(
            (
                largest,
                jnp.sum(powers, axis=0, keepdims=True),
                jnp.dot(value, powers.astype(jnp.bfloat16), preferred_element_type=jnp.float32),
            )
        )

    def step(chunk, state):
        scores, values = scores_of(chunk)
        after = []
        for (largest, total, kept), score, value in zip(state, scores, values):
            now = jnp.maximum(largest, jnp.max(score, axis=0, keepdims=True))
            fade = jnp.exp2(largest - now)
            powers = jnp.exp2(score - now)
            after.append(
                (
                    now,
                    total * fade + jnp.sum(powers, axis=0, keepdims=True),
                    kept * fade
                    + jnp.dot(
                        value, powers.astype(jnp.bfloat16), preferred_element_type=jnp.float32
                    ),
                )
            )
        return tuple(after)

    state = lax.fori_loop(0, me, step, tuple(state))
    for head, (_, total, kept) in enumerate(state):
        out_ref[:, head * nope : (head + 1) * nope] = jnp.transpose(kept / total).astype(
            out_ref.dtype
        )


def attend(me, queries_t, shared, ups, heads_here, nope, channels, scale):
    groups, tokens, width = shared.shape
    columns = heads_here * nope
    depth = queries_t.shape[1]
    return pl.pallas_call(
        functools.partial(attend_kernel, heads_here, nope, channels, scale),
        grid_spec=pltpu.PrefetchScalarGridSpec(
            num_scalar_prefetch=1,
            grid=(groups,),
            in_specs=[
                pl.BlockSpec((heads_here, depth, tokens), lambda g, me: (g, 0, 0)),
                pl.BlockSpec((groups, tokens, width), lambda g, me: (0, 0, 0)),
                pl.BlockSpec((ups.shape[0], 1) + ups.shape[2:], lambda g, me: (0, g, 0, 0)),
            ],
            out_specs=pl.BlockSpec((tokens, columns), lambda g, me: (0, g)),
        ),
        out_shape=jax.ShapeDtypeStruct((tokens, groups * columns), jnp.bfloat16),
        cost_estimate=pl.CostEstimate(
            flops=20 * groups * tokens * groups * tokens * columns,
            bytes_accessed=2 * groups * tokens * width,
            transcendentals=0,
        ),
    )(me, queries_t, shared, ups)


def project_kernel(heads_ref, weight_ref, resid_ref, gain_ref, after_ref, normed_ref, square_ref):
    part = pl.program_id(0)
    rows, width = weight_ref.shape[0] * weight_ref.shape[2], weight_ref.shape[3]
    weight = weight_ref[...].reshape(rows, width)
    projected = (
        jnp.dot(heads_ref[...], weight, preferred_element_type=jnp.float32)
        .astype(jnp.bfloat16)
        .astype(jnp.float32)
    )
    after = resid_ref[...].astype(jnp.float32) + projected
    after_ref[part] = after

    @pl.when(part == 0)
    def _():
        square_ref[...] = jnp.zeros_like(square_ref)

    square_ref[...] += jnp.sum(after * after, axis=1, keepdims=True)

    @pl.when(part == pl.num_programs(0) - 1)
    def _():
        parts = after_ref.shape[0]
        factor = lax.rsqrt(square_ref[...] / (parts * width) + epsilon)
        for at in range(parts):
            cols = slice(at * width, (at + 1) * width)
            normed_ref[:, cols] = (after_ref[at] * factor * gain_ref[:, cols]).astype(
                normed_ref.dtype
            )


def project(heads, weights, resid, gain):
    groups, parts, rows, width = weights.shape
    tokens = heads.shape[0]
    return pl.pallas_call(
        project_kernel,
        grid=(parts,),
        in_specs=[
            pl.BlockSpec((tokens, groups * rows), lambda p: (0, 0)),
            pl.BlockSpec((groups, 1, rows, width), lambda p: (0, p, 0, 0)),
            pl.BlockSpec((tokens, width), lambda p: (0, p)),
            pl.BlockSpec((1, parts * width), lambda p: (0, 0)),
        ],
        out_specs=[
            pl.BlockSpec((parts, tokens, width), lambda p: (0, 0, 0)),
            pl.BlockSpec((tokens, parts * width), lambda p: (0, 0)),
        ],
        out_shape=[
            jax.ShapeDtypeStruct((parts, tokens, width), jnp.float32),
            jax.ShapeDtypeStruct((tokens, parts * width), jnp.bfloat16),
        ],
        scratch_shapes=[pltpu.VMEM((tokens, 1), jnp.float32)],
        cost_estimate=pl.CostEstimate(
            flops=2 * tokens * groups * rows * parts * width,
            bytes_accessed=2 * groups * rows * parts * width,
            transcendentals=0,
        ),
    )(heads, weights, resid, gain)


def gather_kernel(
    outer, inner, dp_count, row_ref, piece_ref, rows_ref, pieces_ref,
    own_sems, far_send, far_recv, near_send, near_recv, dp_send, dp_recv,
):
    me = lax.axis_index("sp")
    dp = lax.axis_index("dp")
    far, near = me // inner, lax.rem(me, inner)
    barrier = pltpu.get_barrier_semaphore()
    fars = [lax.rem(far + step, outer) for step in range(1, outer)]
    nears = [lax.rem(near + step, inner) for step in range(1, inner)]
    dps = [lax.rem(dp + step, dp_count) for step in range(1, dp_count)]
    greeted = (
        [{"sp": f * inner + near} for f in fars]
        + [{"sp": far * inner + n} for n in nears]
        + [{"dp": d} for d in dps]
    )
    for peer in greeted:
        pl.semaphore_signal(barrier, inc=1, device_id=peer, device_id_type=pl.DeviceIdType.MESH)
    pl.semaphore_wait(barrier, len(greeted))

    def remote(source, target, send, recv, peer):
        copy = pltpu.make_async_remote_copy(
            src_ref=source, dst_ref=target, send_sem=send, recv_sem=recv,
            device_id=peer, device_id_type=pl.DeviceIdType.MESH,
        )
        copy.start()
        return copy

    def pair(row, piece, block, send, recv, peer):
        return [
            remote(row, rows_ref.at[block], send.at[0], recv.at[0], peer),
            remote(piece, pieces_ref.at[dp, block], send.at[1], recv.at[1], peer),
        ]

    out_far = []
    for at, f in enumerate(fars):
        out_far.append(pair(row_ref, piece_ref, me, far_send.at[at], far_recv.at[at], {"sp": f * inner + near}))
    last = []

    def share(block):
        for at, d in enumerate(dps):
            last.append(
                remote(
                    pieces_ref.at[dp, block], pieces_ref.at[dp, block],
                    dp_send.at[len(last)], dp_recv.at[len(last)], {"dp": d},
                )
            )

    sends = []
    for at, n in enumerate(nears):
        sends.append(pair(row_ref, piece_ref, me, near_send.at[0, at], near_recv.at[0, at], {"sp": far * inner + n}))
    own = [
        pltpu.make_async_copy(row_ref, rows_ref.at[me], own_sems.at[0]),
        pltpu.make_async_copy(piece_ref, pieces_ref.at[dp, me], own_sems.at[1]),
    ]
    for copy in own:
        copy.start()
    for copy in own:
        copy.wait()
    share(me)
    for at in range(outer - 1):
        for copy in out_far[at]:
            copy.wait_recv()
        block = lax.rem(far + outer - 1 - at, outer) * inner + near
        for to, n in enumerate(nears):
            sends.append(
                pair(
                    rows_ref.at[block], pieces_ref.at[dp, block], block,
                    near_send.at[at + 1, to], near_recv.at[at + 1, to], {"sp": far * inner + n},
                )
            )
        share(block)
    for at in range(outer):
        for to in range(inner - 1):
            for copy in sends[at * (inner - 1) + to]:
                copy.wait_recv()
            column = lax.rem(near + inner - 1 - to, inner)
            share(lax.rem(far + outer - at, outer) * inner + column)
    for copies in out_far + sends:
        for copy in copies:
            copy.wait_send()
    for copy in last:
        copy.wait()


def gather_shared(row, piece, sp_count, dp_count, number):
    inner = max(d for d in range(1, math.isqrt(sp_count) + 1) if sp_count % d == 0)
    outer = sp_count // inner
    dma = pltpu.SemaphoreType.DMA
    return pl.pallas_call(
        functools.partial(gather_kernel, outer, inner, dp_count),
        out_shape=[
            jax.ShapeDtypeStruct((sp_count,) + row.shape, row.dtype),
            jax.ShapeDtypeStruct((dp_count, sp_count) + piece.shape, piece.dtype),
        ],
        in_specs=[pl.BlockSpec(memory_space=pltpu.VMEM)] * 2,
        out_specs=[pl.BlockSpec(memory_space=pltpu.VMEM)] * 2,
        scratch_shapes=[
            dma((2,)),
            dma((max(outer - 1, 1), 2)),
            dma((max(outer - 1, 1), 2)),
            dma((outer, max(inner - 1, 1), 2)),
            dma((outer, max(inner - 1, 1), 2)),
            dma((max(dp_count - 1, 1) * sp_count,)),
            dma((max(dp_count - 1, 1) * sp_count,)),
        ],
        compiler_params=pltpu.CompilerParams(collective_id=number, has_side_effects=True),
        cost_estimate=pl.CostEstimate(flops=2 * 10**10, bytes_accessed=10**7, transcendentals=0),
    )(row, piece)


def in_three(values):
    high = lax.reduce_precision(values, 8, 7)
    middle = lax.reduce_precision(values - high, 8, 7)
    low = values - high - middle
    return [piece.astype(jnp.bfloat16) for piece in (high, middle, low)]


def shards(
    query_nope,
    query_rope,
    latent,
    key_rope,
    resid,
    latent_gain,
    key_up,
    value_up,
    out_proj,
    norm_gain,
    expert_gate,
    expert_up,
    expert_down,
    routes,
    route_weight,
):
    tokens, channels = latent.shape[1:]
    sp_count = lax.axis_size("sp")
    dp_count = lax.axis_size("dp")
    me = lax.axis_index("sp")
    nope, rope = query_nope.shape[-1], query_rope.shape[-1]
    heads_here = key_up.shape[1] // nope
    scale = (nope + rope) ** (-0.5)
    local_pos = me * tokens + jnp.arange(tokens, dtype=jnp.int32)
    latent_normed = rms_scaled(latent[0], latent_gain).astype(jnp.bfloat16)
    key_turned = rotate(key_rope[0], local_pos)
    spare = 128 - rope
    row = jnp.concatenate(
        [latent_normed, key_turned, jnp.zeros((tokens, spare), jnp.bfloat16)], axis=1
    )
    piece = channels // dp_count
    ups = lax.dynamic_slice_in_dim(
        jnp.concatenate([key_up, value_up], axis=1), lax.axis_index("dp") * piece, piece, axis=0
    )
    shared, ups = gather_shared(row, ups, sp_count, dp_count, 0)
    weights = lax.all_gather(out_proj, ("sp", "dp"), axis=0)
    weights = weights.reshape(sp_count, dp_count, *out_proj.shape)
    query_turned = rotate(query_rope[0], local_pos)
    queries = jnp.concatenate(
        [query_nope[0], query_turned, jnp.zeros(query_turned.shape[:2] + (128 - rope,), jnp.bfloat16)],
        axis=-1,
    )
    queries_t = jnp.transpose(queries, (1, 2, 0))
    heads = attend(
        me.astype(jnp.int32)[None], queries_t, shared, ups, heads_here, nope, channels, scale
    )
    after, normed = project(heads, weights, resid[0], norm_gain[None])

    experts_all = sp_count * expert_gate.shape[0]
    capacity = 4 * tokens // experts_all
    ids = jnp.arange(experts_all, dtype=jnp.int32)[:, None, None]
    mine = routes[0][None] == ids
    named = jnp.any(mine, axis=-1)
    weight = jnp.sum(jnp.where(mine, route_weight[0][None], 0.0), axis=-1)
    place = jnp.cumsum(named.astype(jnp.int32), axis=1) - 1
    chosen = (
        place[:, None, :] == jnp.arange(capacity, dtype=jnp.int32)[None, :, None]
    ) & named[:, None, :]
    select = chosen.astype(jnp.bfloat16).reshape(experts_all * capacity, tokens)
    outgoing = jnp.dot(select, normed, preferred_element_type=jnp.float32).astype(jnp.bfloat16)
    rows = lax.all_to_all(outgoing, "sp", split_axis=0, concat_axis=0, tiled=True)
    gate = jnp.dot(rows, expert_gate[0], preferred_element_type=jnp.float32)
    upward = jnp.dot(rows, expert_up[0], preferred_element_type=jnp.float32)
    hidden = (jax.nn.silu(gate) * upward).astype(jnp.bfloat16)
    result = jnp.dot(hidden, expert_down[0], preferred_element_type=jnp.float32).astype(
        jnp.bfloat16
    )
    returned = lax.all_to_all(result, "sp", split_axis=0, concat_axis=0, tiled=True)
    mixing = jnp.where(chosen, weight[:, None, :], 0.0).reshape(experts_all * capacity, tokens)
    routed = sum(
        lax.dot_general(part, returned, (((0,), (0,)), ((), ())), preferred_element_type=jnp.float32)
        for part in in_three(mixing)[0:2]
    )
    after = jnp.concatenate([after[p] for p in range(dp_count)], axis=1)
    return (after + routed).astype(jnp.bfloat16)[None]


def solution(mesh):
    return jax.shard_map(
        shards,
        mesh=mesh,
        in_specs=(
            P("dp", "sp", None, None),
            P("dp", "sp", None, None),
            P("dp", "sp", None),
            P("dp", "sp", None),
            P("dp", "sp", None),
            P(),
            P(None, "sp"),
            P(None, "sp"),
            P("sp", "dp"),
            P(),
            P("sp", None, None),
            P("sp", None, None),
            P("sp", None, None),
            P("dp", "sp", None),
            P("dp", "sp", None),
        ),
        out_specs=P("dp", "sp", None),
        check_vma=False,
    )
```

profile of v0, /device:TPU:0, one launch (start us, length us, event | category | flops | bytes accessed | tf_op | source)
XLA Modules:
  0.0 361.5 jit_solution(12690636377496625040)
XLA Ops:
  6.5 0.7 all-gather.3.cloned.1.call-update
  7.3 0.1 pad.13.clone
  7.4 0.1 pad.9.clone
  7.4 0.9 copy.40
  8.4 0.6 subtract_convert_fusion.1
  9.0 0.1 copy.39
  9.1 1.6 copy.36
  10.7 0.7 fusion.32
  11.4 0.6 reduce-window.6
  12.0 0.2 slice_reduce_fusion
  12.3 0.3 fusion.18
  12.6 1.4 fusion.31.piece_ref
  14.0 0.1 fusion.28
  14.1 0.1 fusion.30
  14.3 0.8 maximum_maximum_fusion.row_ref
  15.0 0.1 bitcast_convert_fusion
  15.1 0.2 subtract_convert_fusion
  15.3 2.0 maximum_bitcast_fusion.query_ref
  17.3 57.0 %shard_map.145 = (bf16[8,256,384]{2,1,0:T(8,128)(2,1)}, bf16[4,8,64,512]{3,2,1,0:T(8,128)(2,1)}) custom-call(bf16[256,384]{1,0:T(8,128)(2,1)} %maximum_maximum_fusion.row_ref, bf16[64,512]{1,0:T(8,128)(2,1)} %fusion.31.piece_ref), custom_call_target="tpu_custom_call" | custom-call | flops 20000000000 | bytes 10000000 | tf_op jit(solution)/shard_map/pallas_call | solution.py:285
  74.3 9.2 %shard_map.146.heads_ref = bf16[256,2048]{1,0:T(8,128)(2,1)} custom-call(s32[1]{0:T(128)} %bitcast.me_ref, bf16[16,256,256]{2,1,0:T(8,128)(2,1)} %maximum_bitcast_fusion.query_ref, bf16[8,256,384]{2,1,0:T(8,128)(2,1)} %get-tuple-element.9.shared_ref, bf16[4,8,64,512]{3,2,1,0:T(8,128)(2,1)} %get-tuple-element.10.ups_ref), custom_call_target="tpu_custom_call" | custom-call | flops 21474836480 | bytes 1572864 | tf_op jit(solution)/shard_map/pallas_call | solution.py:117
  83.5 27.4 %all-gather.3.cloned.1.call-done = bf16[8192,512]{1,0:T(8,128)(2,1)} async-done(((bf16[256,512]{1,0:T(8,128)(2,1)}), bf16[8192,512]{1,0:T(8,128)(2,1)}) %all-gather.3.cloned.1.call-update) | async-done | bytes 8388624 | tf_op jit(solution)/shard_map/all_gather | solution.py:350
  111.0 8.2 %shard_map.147 = (f32[4,256,512]{2,1,0:T(8,128)}, bf16[256,2048]{1,0:T(8,128)(2,1)}) custom-call(bf16[256,2048]{1,0:T(8,128)(2,1)} %shard_map.146.heads_ref, bf16[8,4,256,512]{3,2,1,0:T(8,128)(2,1)} %bitcast.77, bf16[256,2048]{1,0:T(8,128)(2,1)} %bitcast.82, f32[1,2048]{1,0:T(1,128)} %bitcast.85), custom_call_target="tpu_custom_call" | custom-call | flops 2147483648 | bytes 8388608 | tf_op jit(solution)/shard_map/pallas_call | solution.py:170
  119.2 2.5 convolution_convert_fusion
  121.7 111.2 %all_to_all.21 = bf16[8,128,2048]{2,1,0:T(8,128)(2,1)S(1)} all-to-all(bf16[8,128,2048]{2,1,0:T(8,128)(2,1)S(1)} %bitcast.76), channel_id=1, replica_groups=mesh['sp'=8,'dp'=4] {'sp'}, dimensions={0} | all-to-all | bytes 8388608 | tf_op jit(solution)/shard_map/all_to_all | solution.py:375
  233.0 4.5 %fusion.2 = f32[1024,1024]{1,0:T(8,128)S(1)} fusion(bf16[1024,2048]{1,0:T(8,128)(2,1)S(1)} %bitcast.79, bf16[1,2048,1024]{2,1,0:T(8,128)(2,1)S(1)} %copy-done.8), kind=kOutput, calls=%fused_computation.2 | convolution fusion | flops 4294967296 | bytes 12582912 | tf_op jit(solution)/shard_map/dot_general | solution.py:377
  237.5 5.4 %multiply_convert_fusion = bf16[1024,1024]{1,0:T(8,128)(2,1)S(1)} fusion(f32[1024,1024]{1,0:T(8,128)S(1)} %fusion.2, bf16[1024,2048]{1,0:T(8,128)(2,1)S(1)} %bitcast.80, bf16[1,2048,1024]{2,1,0:T(8,128)(2,1)S(1)} %copy-done.9), kind=kOutput, calls=%fused_computation.6 | convolution fusion | flops 4301258752 | bytes 14680064 | tf_op jit(solution)/shard_map/dot_general | solution.py:376
  242.9 6.1 %fusion.6 = bf16[1024,2048]{1,0:T(8,128)(2,1)} fusion(bf16[1024,1024]{1,0:T(8,128)(2,1)S(1)} %multiply_convert_fusion, bf16[1,1024,2048]{2,1,0:T(8,128)(2,1)S(1)} %copy-done.10), kind=kOutput, calls=%fused_computation.8 | convolution fusion | flops 4297064448 | bytes 10485760 | tf_op jit(solution)/shard_map/dot_general | solution.py:379
  249.0 4.7 %all-to-all-start.1 = ((bf16[8,128,2048]{2,1,0:T(8,128)(2,1)}), bf16[8,128,2048]{2,1,0:T(8,128)(2,1)}, u32[]{:S(2)}, u32[]{:S(2)}) async-start(bf16[8,128,2048]{2,1,0:T(8,128)(2,1)} %bitcast.78), calls=%async_computation.1 | async-start | bytes 8388608 | tf_op jit(solution)/shard_map/all_to_all | solution.py:382
  253.7 1.3 slice_bitcast_fusion.3
  255.0 91.7 %all-to-all-done.1 = bf16[8,128,2048]{2,1,0:T(8,128)(2,1)} async-done(((bf16[8,128,2048]{2,1,0:T(8,128)(2,1)}), bf16[8,128,2048]{2,1,0:T(8,128)(2,1)}, u32[]{:S(2)}, u32[]{:S(2)}) %all-to-all-start.1) | async-done | bytes 4194336 | tf_op jit(solution)/shard_map/all_to_all | solution.py:382
  346.6 3.5 convolution_bitcast_fusion
  350.2 4.5 %fusion.14 = bf16[1,256,2048]{2,1,0:T(8,128)(2,1)} fusion(f32[256,2048]{1,0:T(8,128)S(1)} %convolution_bitcast_fusion, bf16[8,128,2048]{2,1,0:T(8,128)(2,1)} %all-to-all-done.1, f32[256,512]{1,0:T(8,128)S(1)} %get-tuple-element.14, f32[256,512]{1,0:T(8,128)S(1)} %copy-done.1, f32[256,512]{1,0:T(8,128)S(1)} %copy-done.2, ...), kind=kOutput, calls=%fused_computation.14 | convolution fusion | flops 1078198272 | bytes 9455616 | tf_op jit(solution)/shard_map/dot_general | solution.py:385
  (35 shorter events, 0.3 us)
Async XLA Ops:
  6.5 7.5 %copy-start.4 = (bf16[1,256,256]{2,1,0:T(8,128)(2,1)S(1)}, bf16[1,256,256]{2,1,0:T(8,128)(2,1)}, u32[]{:S(2)}) copy-start(bf16[1,256,256]{2,1,0:T(8,128)(2,1)} %param.17) | copy-start | bytes 393220
  6.5 7.6 %copy-start.7 = (f32[256]{0:T(256)S(1)}, f32[256]{0:T(256)}, u32[]{:S(2)}) copy-start(f32[256]{0:T(256)} %param.20) | copy-start | bytes 3076
  6.5 8.5 %copy-start.3 = (bf16[1,256,16,64]{1,3,2,0:T(8,128)(2,1)S(1)}, bf16[1,256,16,64]{1,3,2,0:T(8,128)(2,1)}, u32[]{:S(2)}) copy-start(bf16[1,256,16,64]{1,3,2,0:T(8,128)(2,1)} %param.16) | copy-start | bytes 1572868
  6.5 104.4 %all-gather.3.cloned.1.call-start = ((), (), s32[]{:S(2)}) async-start(), calls=%async_computation.2 | async-start | bytes 8650752 | tf_op jit(solution)/shard_map/all_gather | solution.py:350
  121.7 111.3 %copy-start.8 = (bf16[1,2048,1024]{2,1,0:T(8,128)(2,1)S(1)}, bf16[1,2048,1024]{2,1,0:T(8,128)(2,1)}, u32[]{:S(2)}) copy-start(bf16[1,2048,1024]{2,1,0:T(8,128)(2,1)} %param.26) | copy-start | bytes 12582916
  233.0 4.5 %copy-start.9 = (bf16[1,2048,1024]{2,1,0:T(8,128)(2,1)S(1)}, bf16[1,2048,1024]{2,1,0:T(8,128)(2,1)}, u32[]{:S(2)}) copy-start(bf16[1,2048,1024]{2,1,0:T(8,128)(2,1)} %param.25) | copy-start | bytes 12582916
  237.5 5.4 %copy-start.10 = (bf16[1,1024,2048]{2,1,0:T(8,128)(2,1)S(1)}, bf16[1,1024,2048]{2,1,0:T(8,128)(2,1)}, u32[]{:S(2)}) copy-start(bf16[1,1024,2048]{2,1,0:T(8,128)(2,1)} %param.27) | copy-start | bytes 12582916
  249.0 4.7 %copy-start.5 = (s32[1,256,2]{1,2,0:T(2,128)S(1)}, s32[1,256,2]{1,2,0:T(2,128)}, u32[]{:S(2)}) copy-start(s32[1,256,2]{1,2,0:T(2,128)} %param.28) | copy-start | bytes 6148
  249.0 4.7 %copy-start.6 = (f32[1,256,2]{1,2,0:T(2,128)S(1)}, f32[1,256,2]{1,2,0:T(2,128)}, u32[]{:S(2)}) copy-start(f32[1,256,2]{1,2,0:T(2,128)} %param.29) | copy-start | bytes 6148
  249.0 4.7 %copy-start = (f32[4,256,512]{2,1,0:T(8,128)S(1)}, f32[4,256,512]{2,1,0:T(8,128)}, u32[]{:S(2)}) copy-start(f32[4,256,512]{2,1,0:T(8,128)} %get-tuple-element.11) | copy-start | bytes 6291460
  249.0 97.7 %all-to-all-start.1 = ((bf16[8,128,2048]{2,1,0:T(8,128)(2,1)}), bf16[8,128,2048]{2,1,0:T(8,128)(2,1)}, u32[]{:S(2)}, u32[]{:S(2)}) async-start(bf16[8,128,2048]{2,1,0:T(8,128)(2,1)} %bitcast.78), calls=%async_computation.1 | async-start | bytes 8388608 | tf_op jit(solution)/shard_map/all_to_all | solution.py:382
  254.9 95.2 %copy-start.1 = (f32[256,512]{1,0:T(8,128)S(1)}, f32[256,512]{1,0:T(8,128)}, u32[]{:S(2)}) copy-start(f32[256,512]{1,0:T(8,128)} %get-tuple-element.15) | copy-start | bytes 1572868
  254.9 95.2 %copy-start.2 = (f32[256,512]{1,0:T(8,128)S(1)}, f32[256,512]{1,0:T(8,128)}, u32[]{:S(2)}) copy-start(f32[256,512]{1,0:T(8,128)} %get-tuple-element.16) | copy-start | bytes 1572868
Sparse Core Ops, SparseCore 0:
  10.2 100.7 all-gather.2
where the time goes:
time: 362 us; the launch traced here: 361 us
  waiting for transfers between devices  120 us (33%)
  blocking collectives  111 us (31%)
  Pallas kernels  74.5 us (21%)
  matrix products  26.4 us (7%)
  between operations  13.6 us (4%)
  other arithmetic  6.87 us (2%)
  starting transfers between devices  4.68 us (1%)
  local copies, waits for them, and re-layouts  4.33 us (1%)
    all_to_all x1, blocking collectives, shards(): lax.all_to_all(outgoing, 'sp', split_axis=0, concat_axis=0, tiled=True)  111 us
    all_to_all x1, waiting for transfers between devices, shards(): lax.all_to_all(result, 'sp', split_axis=0, concat_axis=0, tiled=True)  91.7 us
    pallas_call x1, Pallas kernels, gather_shared(): pl.pallas_call(functools.partial(gather_kernel, outer, inner, dp_count),...  57 us
    all_gather x1, waiting for transfers between devices, shards(): weights = lax.all_gather(out_proj, ('sp', 'dp'), axis=0)  27.4 us
    pallas_call x1, Pallas kernels, attend(): pl.pallas_call(functools.partial(attend_kernel, heads_here, nope, channel...  9.22 us
    pallas_call x1, Pallas kernels, project(): pl.pallas_call(project_kernel, grid=(parts,), in_specs=[pl.BlockSpec((tok...  8.24 us
    dot_general x2, matrix products, shards(): lax.dot_general(part, returned, (((0,), (0,)), ((), ())), preferred_eleme...  7.99 us
  transfers between devices with their start and end apart: 2, of which 2 were waited for; matrix products, arithmetic and copies ran while one was open for 3% of the time, Pallas kernels for 18%

commit v1 on v0

--- a/solution.py
+++ b/solution.py
@@ -159,9 +159,7 @@
         factor = lax.rsqrt(square_ref[...] / (parts * width) + epsilon)
         for at in range(parts):
             cols = slice(at * width, (at + 1) * width)
-            normed_ref[:, cols] = (after_ref[at] * factor * gain_ref[:, cols]).astype(
-                normed_ref.dtype
-            )
+            normed_ref[at] = (after_ref[at] * factor * gain_ref[:, cols]).astype(normed_ref.dtype)
 
 
 def project(heads, weights, resid, gain):
@@ -178,11 +176,11 @@
         ],
         out_specs=[
             pl.BlockSpec((parts, tokens, width), lambda p: (0, 0, 0)),
-            pl.BlockSpec((tokens, parts * width), lambda p: (0, 0)),
+            pl.BlockSpec((parts, tokens, width), lambda p: (0, 0, 0)),
         ],
         out_shape=[
             jax.ShapeDtypeStruct((parts, tokens, width), jnp.float32),
-            jax.ShapeDtypeStruct((tokens, parts * width), jnp.bfloat16),
+            jax.ShapeDtypeStruct((parts, tokens, width), jnp.bfloat16),
         ],
         scratch_shapes=[pltpu.VMEM((tokens, 1), jnp.float32)],
         cost_estimate=pl.CostEstimate(
@@ -279,8 +277,7 @@
 
 
 def gather_shared(row, piece, sp_count, dp_count, number):
-    inner = max(d for d in range(1, math.isqrt(sp_count) + 1) if sp_count % d == 0)
-    outer = sp_count // inner
+    outer, inner = split_of(sp_count)
     dma = pltpu.SemaphoreType.DMA
     return pl.pallas_call(
         functools.partial(gather_kernel, outer, inner, dp_count),
@@ -304,11 +301,326 @@
     )(row, piece)
 
 
-def in_three(values):
-    high = lax.reduce_precision(values, 8, 7)
-    middle = lax.reduce_precision(values - high, 8, 7)
-    low = values - high - middle
-    return [piece.astype(jnp.bfloat16) for piece in (high, middle, low)]
+def split_of(sp_count):
+    inner = max(d for d in range(1, math.isqrt(sp_count) + 1) if sp_count % d == 0)
+    return sp_count // inner, inner
+
+
+def experts_kernel(
+    outer, inner, capacity,
+    normed_ref, meta_ref, after_ref, gate_hbm, up_hbm, down_hbm, out_ref,
+    gate_w, up_w, down_w, blocks, metas, picked, rows, made, back, partial, coming, total, gate_acc, up_acc,
+    weight_sems, meta_send, meta_recv, block_send, block_recv, row_send, row_recv,
+    back_send, back_recv, sum_send, sum_recv,
+):
+    me = lax.axis_index("sp")
+    z, y = me // inner, lax.rem(me, inner)
+    parts, tokens, width = normed_ref.shape
+    slots = inner * capacity
+    loads = [
+        pltpu.make_async_copy(hbm.at[0], ref, weight_sems.at[at])
+        for at, (hbm, ref) in enumerate([(gate_hbm, gate_w), (up_hbm, up_w), (down_hbm, down_w)])
+    ]
+    for load in loads:
+        load.start()
+
+    barrier = pltpu.get_barrier_semaphore()
+    steps_z = [lax.rem(z + step, outer) for step in range(1, outer)]
+    steps_y = [lax.rem(y + step, inner) for step in range(1, inner)]
+    greeted = [{"sp": at * inner + y} for at in steps_z] + [{"sp": z * inner + at} for at in steps_y]
+    for peer in greeted:
+        pl.semaphore_signal(barrier, inc=1, device_id=peer, device_id_type=pl.DeviceIdType.MESH)
+    pl.semaphore_wait(barrier, len(greeted))
+
+    def remote(source, target, send, recv, at_z, at_y):
+        return pltpu.make_async_remote_copy(
+            src_ref=source, dst_ref=target, send_sem=send, recv_sem=recv,
+            device_id={"sp": at_z * inner + at_y}, device_id_type=pl.DeviceIdType.MESH,
+        )
+
+    def block_copy(source, part, own, way):
+        ref = normed_ref.at[part] if own else blocks.at[source, part]
+        return remote(
+            ref, blocks.at[source, part],
+            block_send.at[(way + 1) // 2, source, part], block_recv.at[source, part], z + way, y,
+        )
+
+    def meta_copy(step):
+        at = lax.rem(z + step, outer)
+        return remote(meta_ref.at[at], metas.at[z], meta_send.at[step - 1], meta_recv.at[z], at, y)
+
+    def row_copy(source, step, part):
+        at = lax.rem(y + step, inner)
+        return remote(
+            picked.at[source, at, part], rows.at[source, y, part],
+            row_send.at[source, step - 1, part], row_recv.at[source, y, part], z, at,
+        )
+
+    def back_copy(source, step, part):
+        at = lax.rem(y + step, inner)
+        return remote(
+            made.at[source, at, part], back.at[source, y, part],
+            back_send.at[source, step - 1, part], back_recv.at[source, y, part], z, at,
+        )
+
+    def sum_copy(source, part, way):
+        slot = source if way < 0 else jnp.where(source == z + 1, outer, source)
+        return remote(
+            partial.at[source, part], coming.at[slot, part],
+            sum_send.at[source, part], sum_recv.at[slot, part], z + way, y,
+        )
+
+    def wait_recv(ref, sem):
+        remote(ref, ref, block_send.at[0, 0, 0], sem, z, y).wait_recv()
+
+    for step in range(1, outer):
+        meta_copy(step).start()
+    for part in range(parts):
+        for way in (1, -1):
+
+            @pl.when((z + way >= 0) & (z + way < outer))
+            def _():
+                block_copy(z, part, True, way).start()
+
+    blocks[z] = normed_ref[...]
+    metas[z] = meta_ref[z]
+
+    orders = [sorted(range(outer), key=lambda s: (abs(s - at), s)) for at in range(outer)]
+
+    def source_of(turn):
+        found = jnp.int32(0)
+        for at in range(outer):
+            for index in range(outer):
+                found = jnp.where((z == at) & (turn == index), orders[at][index], found)
+        return found
+
+    def forwards(source):
+        return [
+            (1, (source < z) & (z < outer - 1)),
+            (-1, (source > z) & (z > 0)),
+        ]
+
+    def ends(source):
+        return [
+            (-1, (source < z) & (z == outer - 1)),
+            (1, (source > z) & (z == 0)),
+        ]
+
+    def turn_body(turn, carry):
+        source = source_of(turn)
+
+        @pl.when(turn > 0)
+        def _():
+            wait_recv(metas.at[source], meta_recv.at[source])
+
+        meta = metas[source]
+        slot_ids = lax.broadcasted_iota(jnp.int32, (capacity, tokens), 0).astype(jnp.float32)
+        select = jnp.concatenate(
+            [
+                jnp.where(meta[at : at + 1, :] == slot_ids, 1.0, 0.0).astype(jnp.bfloat16)
+                for at in range(inner)
+            ],
+            axis=0,
+        )
+
+        def pick(part, carry):
+            @pl.when(turn > 0)
+            def _():
+                wait_recv(blocks.at[source, part], block_recv.at[source, part])
+
+            for way, needed in forwards(source):
+
+                @pl.when(needed)
+                def _():
+                    block_copy(source, part, False, way).start()
+
+            found = jnp.dot(
+                select, blocks[source, part], preferred_element_type=jnp.float32
+            ).astype(jnp.bfloat16)
+            for at in range(inner):
+                picked[source, at, part] = found[at * capacity : (at + 1) * capacity]
+            rows[source, y, part] = picked[source, y, part]
+            for step in range(1, inner):
+                row_copy(source, step, part).start()
+            return carry
+
+        lax.fori_loop(0, parts, pick, 0)
+
+        @pl.when(turn == 0)
+        def _():
+            for load in loads:
+                load.wait()
+
+        gate_acc[...] = jnp.zeros_like(gate_acc)
+        up_acc[...] = jnp.zeros_like(up_acc)
+
+        def widen(part, carry):
+            for step in range(1, inner):
+                at = lax.rem(y + step, inner)
+                wait_recv(rows.at[source, at, part], row_recv.at[source, at, part])
+            taken = jnp.concatenate([rows[source, at, part] for at in range(inner)], axis=0)
+            depth = pl.ds(pl.multiple_of(part * width, width), width)
+            gate_acc[...] += jnp.dot(taken, gate_w[depth, :], preferred_element_type=jnp.float32)
+            up_acc[...] += jnp.dot(taken, up_w[depth, :], preferred_element_type=jnp.float32)
+            return carry
+
+        lax.fori_loop(0, parts, widen, 0)
+        gate = gate_acc[...]
+        hidden = (gate / (1.0 + jnp.exp(-gate)) * up_acc[...]).astype(jnp.bfloat16)
+
+        for part in range(parts):
+            cols = slice(part * width, (part + 1) * width)
+            result = jnp.dot(hidden, down_w[:, cols], preferred_element_type=jnp.float32).astype(
+                jnp.bfloat16
+            )
+            for at in range(inner):
+                made[source, at, part] = result[at * capacity : (at + 1) * capacity]
+            back[source, y, part] = made[source, y, part]
+            for step in range(1, inner):
+                back_copy(source, step, part).start()
+
+        columns = jnp.transpose(meta)
+        slot_lanes = lax.broadcasted_iota(jnp.int32, (tokens, capacity), 1).astype(jnp.float32)
+        spread = [
+            jnp.where(columns[:, at : at + 1] == slot_lanes, 1.0, 0.0).astype(jnp.bfloat16)
+            for at in range(inner)
+        ]
+
+        def gather_back(part, carry):
+            for step in range(1, inner):
+                at = lax.rem(y + step, inner)
+                wait_recv(back.at[source, at, part], back_recv.at[source, at, part])
+            summed = sum(
+                jnp.dot(spread[at], back[source, at, part], preferred_element_type=jnp.float32)
+                * columns[:, inner + at : inner + at + 1]
+                for at in range(inner)
+            )
+
+            @pl.when(turn == 0)
+            def _():
+                total[part] = after_ref[part] + summed
+
+            @pl.when(turn > 0)
+            def _():
+                partial[source, part] = summed.astype(jnp.bfloat16)
+
+            for way, needed in ends(source):
+
+                @pl.when(needed)
+                def _():
+                    sum_copy(source, part, way).start()
+
+            return carry
+
+        lax.fori_loop(0, parts, gather_back, 0)
+        return carry
+
+    lax.fori_loop(0, outer, turn_body, 0)
+
+    def relay(tick, carry):
+        for way in (-1, 1):
+            since = tick - (z if way > 0 else outer - 1 - z)
+            part = lax.rem(since + parts * outer, parts)
+            steps = (since + parts * outer) // parts - outer
+            source = steps if way > 0 else outer - 1 - steps
+            passing = (source > z) if way > 0 else (source < z)
+            valid = (source >= 0) & (source < outer) & passing & (z - way >= 0) & (z - way < outer)
+
+            @pl.when(valid)
+            def _():
+                wait_recv(coming.at[source, part], sum_recv.at[source, part])
+                partial[source, part] = (
+                    partial[source, part].astype(jnp.float32)
+                    + coming[source, part].astype(jnp.float32)
+                ).astype(jnp.bfloat16)
+                sum_copy(source, part, way).start()
+
+        return carry
+
+    lax.fori_loop(0, outer * (parts + 1), relay, 0)
+
+    for part in range(parts):
+        for slot, valid in ((z, z < outer - 1), (outer, z > 0)):
+
+            @pl.when(valid)
+            def _():
+                wait_recv(coming.at[slot, part], sum_recv.at[slot, part])
+                total[part] += coming[slot, part].astype(jnp.float32)
+
+        out_ref[:, part * width : (part + 1) * width] = total[part].astype(out_ref.dtype)
+
+    for step in range(1, outer):
+        meta_copy(step).wait_send()
+    def drain(source, carry):
+        for part in range(parts):
+            for way in (1, -1):
+                onward = (z + way >= 0) & (z + way < outer)
+                passing = (source == z) | ((source < z) if way > 0 else (source > z))
+
+                @pl.when(onward & passing)
+                def _():
+                    block_copy(source, part, False, way).wait_send()
+
+                @pl.when(onward & ((source > z) if way > 0 else (source < z)))
+                def _():
+                    sum_copy(source, part, way).wait_send()
+
+            for step in range(1, inner):
+                row_copy(source, step, part).wait_send()
+                back_copy(source, step, part).wait_send()
+        return carry
+
+    lax.fori_loop(0, outer, drain, 0)
+
+
+def run_experts(normed, meta, after, gate, up, down, sp_count, capacity, number):
+    outer, inner = split_of(sp_count)
+    parts, tokens, width = normed.shape
+    model, hidden = gate.shape[1:]
+    dma = pltpu.SemaphoreType.DMA
+    bf16, f32 = jnp.bfloat16, jnp.float32
+    steps_y = max(inner - 1, 1)
+    vmem = pl.BlockSpec(memory_space=pltpu.VMEM)
+    anywhere = pl.BlockSpec(memory_space=pl.ANY)
+    return pl.pallas_call(
+        functools.partial(experts_kernel, outer, inner, capacity),
+        out_shape=jax.ShapeDtypeStruct((tokens, parts * width), bf16),
+        in_specs=[vmem, vmem, vmem, anywhere, anywhere, anywhere],
+        out_specs=vmem,
+        scratch_shapes=[
+            pltpu.VMEM((model, hidden), bf16),
+            pltpu.VMEM((model, hidden), bf16),
+            pltpu.VMEM((hidden, model), bf16),
+            pltpu.VMEM((outer, parts, tokens, width), bf16),
+            pltpu.VMEM((outer,) + meta.shape[1:], f32),
+            pltpu.VMEM((outer, inner, parts, capacity, width), bf16),
+            pltpu.VMEM((outer, inner, parts, capacity, width), bf16),
+            pltpu.VMEM((outer, inner, parts, capacity, width), bf16),
+            pltpu.VMEM((outer, inner, parts, capacity, width), bf16),
+            pltpu.VMEM((outer, parts, tokens, width), bf16),
+            pltpu.VMEM((outer + 1, parts, tokens, width), bf16),
+            pltpu.VMEM((parts, tokens, width), f32),
+            pltpu.VMEM((inner * capacity, hidden), f32),
+            pltpu.VMEM((inner * capacity, hidden), f32),
+            dma((3,)),
+            dma((outer,)),
+            dma((outer,)),
+            dma((2, outer, parts)),
+            dma((outer, parts)),
+            dma((outer, steps_y, parts)),
+            dma((outer, inner, parts)),
+            dma((outer, steps_y, parts)),
+            dma((outer, inner, parts)),
+            dma((outer, parts)),
+            dma((outer + 1, parts)),
+        ],
+        compiler_params=pltpu.CompilerParams(
+            collective_id=number, has_side_effects=True, vmem_limit_bytes=60 * 2**20
+        ),
+        cost_estimate=pl.CostEstimate(
+            flops=6 * sp_count * capacity * model * hidden, bytes_accessed=10**7, transcendentals=0
+        ),
+    )(normed, meta, after, gate, up, down)
 
 
 def shards(
@@ -367,26 +679,14 @@
     named = jnp.any(mine, axis=-1)
     weight = jnp.sum(jnp.where(mine, route_weight[0][None], 0.0), axis=-1)
     place = jnp.cumsum(named.astype(jnp.int32), axis=1) - 1
-    chosen = (
-        place[:, None, :] == jnp.arange(capacity, dtype=jnp.int32)[None, :, None]
-    ) & named[:, None, :]
-    select = chosen.astype(jnp.bfloat16).reshape(experts_all * capacity, tokens)
-    outgoing = jnp.dot(select, normed, preferred_element_type=jnp.float32).astype(jnp.bfloat16)
-    rows = lax.all_to_all(outgoing, "sp", split_axis=0, concat_axis=0, tiled=True)
-    gate = jnp.dot(rows, expert_gate[0], preferred_element_type=jnp.float32)
-    upward = jnp.dot(rows, expert_up[0], preferred_element_type=jnp.float32)
-    hidden = (jax.nn.silu(gate) * upward).astype(jnp.bfloat16)
-    result = jnp.dot(hidden, expert_down[0], preferred_element_type=jnp.float32).astype(
-        jnp.bfloat16
-    )
-    returned = lax.all_to_all(result, "sp", split_axis=0, concat_axis=0, tiled=True)
-    mixing = jnp.where(chosen, weight[:, None, :], 0.0).reshape(experts_all * capacity, tokens)
-    routed = sum(
-        lax.dot_general(part, returned, (((0,), (0,)), ((), ())), preferred_element_type=jnp.float32)
-        for part in in_three(mixing)[0:2]
-    )
-    after = jnp.concatenate([after[p] for p in range(dp_count)], axis=1)
-    return (after + routed).astype(jnp.bfloat16)[None]
+    outer, inner = split_of(sp_count)
+    slot = jnp.where(named, place, -1).astype(jnp.float32).reshape(outer, inner, tokens)
+    meta = jnp.concatenate([slot, weight.reshape(outer, inner, tokens)], axis=1)
+    meta = jnp.pad(meta, ((0, 0), (0, -2 * inner % 8), (0, 0)))
+    mixed = run_experts(
+        normed, meta, after, expert_gate, expert_up, expert_down, sp_count, capacity, 1
+    )
+    return mixed[None]
 
 
 def solution(mesh):

time: 362 us -> 297 us (0.82)
  Pallas kernels: 74.5 us -> 248 us
  blocking collectives: 111 us -> 0 us
  waiting for transfers between devices: 120 us -> 22.3 us
  matrix products: 26.4 us -> 0 us
  starting transfers between devices: 4.68 us -> 0.01 us
    pallas_call x0 -> x1, Pallas kernels: none -> 172 us  [run_experts(): pl.pallas_call(functools.partial(experts_kernel, outer, inner, capacity),...]
    all_to_all x1 -> x0, blocking collectives: 111 us -> none  [shards(): lax.all_to_all(outgoing, 'sp', split_axis=0, concat_axis=0, tiled=True)]
    all_to_all x1 -> x0, waiting for transfers between devices: 91.7 us -> none  [shards(): lax.all_to_all(result, 'sp', split_axis=0, concat_axis=0, tiled=True)]
    dot_general x6 -> x0, matrix products: 26.4 us -> none  [the longest x2 7.99 us: shards(): lax.dot_general(part, returned, (((0,), (0,)), ((), ())), preferred_eleme...]
    all_gather x1, waiting for transfers between devices: 27.4 us -> 21.6 us  [shards(): weights = lax.all_gather(out_proj, ('sp', 'dp'), axis=0)]
    all_to_all x1 -> x0, starting transfers between devices: 4.68 us -> none  [shards(): lax.all_to_all(result, 'sp', split_axis=0, concat_axis=0, tiled=True)]
  transfers between devices with their start and end apart: 2 -> 1, of which waited for: 2 -> 1; matrix products, arithmetic and copies ran while one was open for 3% -> 4% of each run, Pallas kernels for 18% -> 23%
where the time goes in v1:
time: 297 us
  Pallas kernels  248 us (84%)
  waiting for transfers between devices  22.3 us (8%)
  between operations  13.5 us (5%)
  other arithmetic  7.98 us (3%)
  local copies, waits for them, and re-layouts  5.39 us (2%)
    pallas_call x1, Pallas kernels, run_experts(): pl.pallas_call(functools.partial(experts_kernel, outer, inner, capacity),...  172 us
    pallas_call x1, Pallas kernels, gather_shared(): pl.pallas_call(functools.partial(gather_kernel, outer, inner, dp_count),...  57.7 us
    all_gather x1, waiting for transfers between devices, shards(): weights = lax.all_gather(out_proj, ('sp', 'dp'), axis=0)  21.6 us
    pallas_call x1, Pallas kernels, attend(): pl.pallas_call(functools.partial(attend_kernel, heads_here, nope, channel...  9.27 us
    pallas_call x1, Pallas kernels, project(): pl.pallas_call(project_kernel, grid=(parts,), in_specs=[pl.BlockSpec((tok...  8.26 us
  transfers between devices with their start and end apart: 1, of which 1 were waited for; matrix products, arithmetic and copies ran while one was open for 4% of the time, Pallas kernels for 23%

profile of v1, /device:TPU:0, one launch (start us, length us, event | category | flops | bytes accessed | tf_op | source)
XLA Modules:
  0.0 296.8 jit_solution(8063237215922691891)
XLA Ops:
  6.5 0.0 copy-start.1
  6.5 0.0 all-gather.3.cloned.1.call-start
  6.5 0.7 all-gather.3.cloned.1.call-update
  7.3 0.1 pad.16.clone
  7.4 0.1 pad.12.clone
  7.4 0.9 copy.39
  8.4 0.6 subtract_convert_fusion.1
  8.9 0.1 copy.37
  9.0 0.1 copy.38
  9.1 1.6 copy.35
  10.7 0.7 fusion.4
  11.4 0.6 reduce-window.6
  12.0 0.2 slice_reduce_fusion
  12.3 0.1 add_add_fusion
  12.4 0.7 select_reduce_fusion
  13.1 0.6 select_maximum_fusion.meta_ref
  13.7 1.4 fusion.3.piece_ref
  15.1 0.0 copy-done.1
  15.1 0.1 fusion
  15.3 0.0 copy-done.2
  15.3 0.1 fusion.2
  15.4 0.8 maximum_maximum_fusion.row_ref
  16.2 0.0 copy-done
  16.2 0.1 bitcast_convert_fusion
  16.3 0.2 subtract_convert_fusion
  16.4 2.0 maximum_bitcast_fusion.query_ref
  18.4 57.7 %shard_map.145 = (bf16[8,256,384]{2,1,0:T(8,128)(2,1)}, bf16[4,8,64,512]{3,2,1,0:T(8,128)(2,1)}) custom-call(bf16[256,384]{1,0:T(8,128)(2,1)} %maximum_maximum_fusion.row_ref, bf16[64,512]{1,0:T(8,128)(2,1)} %fusion.3.piece_ref), custom_call_target="tpu_custom_call" | custom-call | flops 20000000000 | bytes 10000000 | tf_op jit(solution)/shard_map/pallas_call | solution.py:282
  76.2 9.3 %shard_map.146.heads_ref = bf16[256,2048]{1,0:T(8,128)(2,1)} custom-call(s32[1]{0:T(128)} %bitcast.me_ref, bf16[16,256,256]{2,1,0:T(8,128)(2,1)} %maximum_bitcast_fusion.query_ref, bf16[8,256,384]{2,1,0:T(8,128)(2,1)} %get-tuple-element.9.shared_ref, bf16[4,8,64,512]{3,2,1,0:T(8,128)(2,1)} %get-tuple-element.10.ups_ref), custom_call_target="tpu_custom_call" | custom-call | flops 21474836480 | bytes 1572864 | tf_op jit(solution)/shard_map/pallas_call | solution.py:117
  85.4 21.6 %all-gather.3.cloned.1.call-done = bf16[8192,512]{1,0:T(8,128)(2,1)} async-done(((bf16[256,512]{1,0:T(8,128)(2,1)}), bf16[8192,512]{1,0:T(8,128)(2,1)}) %all-gather.3.cloned.1.call-update) | async-done | bytes 8388624 | tf_op jit(solution)/shard_map/all_gather | solution.py:662
  107.0 8.3 %shard_map.147 = (f32[4,256,512]{2,1,0:T(8,128)}, bf16[4,256,512]{2,1,0:T(8,128)(2,1)}) custom-call(bf16[256,2048]{1,0:T(8,128)(2,1)} %shard_map.146.heads_ref, bf16[8,4,256,512]{3,2,1,0:T(8,128)(2,1)} %bitcast.22, bf16[256,2048]{1,0:T(8,128)(2,1)} %bitcast.24, f32[1,2048]{1,0:T(1,128)} %bitcast.28), custom_call_target="tpu_custom_call" | custom-call | flops 2147483648 | bytes 8388608 | tf_op jit(solution)/shard_map/pallas_call | solution.py:168
  115.3 172.4 %shard_map.148 = bf16[256,2048]{1,0:T(8,128)(2,1)} custom-call(bf16[4,256,512]{2,1,0:T(8,128)(2,1)} %get-tuple-element.11.normed_ref, f32[4,8,256]{2,1,0:T(8,128)} %select_maximum_fusion.meta_ref, f32[4,256,512]{2,1,0:T(8,128)} %get-tuple-element.12.after_ref, bf16[1,2048,1024]{2,1,0:T(8,128)(2,1)} %gate_hbm.1, bf16[1,2048,1024]{2,1,0:T(8,128)(2,1)} %up_hbm.1, ...), custom_call_target="tpu_custom_call" | custom-call | flops 12884901888 | bytes 10000000 | tf_op jit(solution)/shard_map/pallas_call | solution.py:585
  287.7 2.3 copy.42
  (15 shorter events, 0.2 us)
Async XLA Ops:
  6.5 8.6 %copy-start.1 = (bf16[1,256,256]{2,1,0:T(8,128)(2,1)S(1)}, bf16[1,256,256]{2,1,0:T(8,128)(2,1)}, u32[]{:S(2)}) copy-start(bf16[1,256,256]{2,1,0:T(8,128)(2,1)} %param.17) | copy-start | bytes 393220
  6.5 8.7 %copy-start.2 = (f32[256]{0:T(256)S(1)}, f32[256]{0:T(256)}, u32[]{:S(2)}) copy-start(f32[256]{0:T(256)} %param.20) | copy-start | bytes 3076
  6.5 9.6 %copy-start = (bf16[1,256,16,64]{1,3,2,0:T(8,128)(2,1)S(1)}, bf16[1,256,16,64]{1,3,2,0:T(8,128)(2,1)}, u32[]{:S(2)}) copy-start(bf16[1,256,16,64]{1,3,2,0:T(8,128)(2,1)} %param.16) | copy-start | bytes 1572868
  6.5 100.5 %all-gather.3.cloned.1.call-start = ((), (), s32[]{:S(2)}) async-start(), calls=%async_computation | async-start | bytes 8650752 | tf_op jit(solution)/shard_map/all_gather | solution.py:662
Sparse Core Ops, SparseCore 0:
  10.2 96.7 all-gather.2

commit v2 on v1

--- a/solution.py
+++ b/solution.py
@@ -310,13 +310,13 @@
     outer, inner, capacity,
     normed_ref, meta_ref, after_ref, gate_hbm, up_hbm, down_hbm, out_ref,
     gate_w, up_w, down_w, blocks, metas, picked, rows, made, back, partial, coming, total, gate_acc, up_acc,
+    select, columns, spread,
     weight_sems, meta_send, meta_recv, block_send, block_recv, row_send, row_recv,
     back_send, back_recv, sum_send, sum_recv,
 ):
     me = lax.axis_index("sp")
     z, y = me // inner, lax.rem(me, inner)
     parts, tokens, width = normed_ref.shape
-    slots = inner * capacity
     loads = [
         pltpu.make_async_copy(hbm.at[0], ref, weight_sems.at[at])
         for at, (hbm, ref) in enumerate([(gate_hbm, gate_w), (up_hbm, up_w), (down_hbm, down_w)])
@@ -406,45 +406,61 @@
             (1, (source > z) & (z == 0)),
         ]
 
-    def turn_body(turn, carry):
+    def needs(source):
+        return functools.reduce(jnp.logical_or, [needed for _, needed in forwards(source)])
+
+    def arrive(source, part):
+        wait_recv(blocks.at[source, part], block_recv.at[source, part])
+
+    def forward(source, part):
+        for way, needed in forwards(source):
+
+            @pl.when(needed)
+            def _():
+                block_copy(source, part, False, way).start()
+
+    def open_turn(turn):
         source = source_of(turn)
 
         @pl.when(turn > 0)
         def _():
             wait_recv(metas.at[source], meta_recv.at[source])
 
-        meta = metas[source]
         slot_ids = lax.broadcasted_iota(jnp.int32, (capacity, tokens), 0).astype(jnp.float32)
-        select = jnp.concatenate(
-            [
-                jnp.where(meta[at : at + 1, :] == slot_ids, 1.0, 0.0).astype(jnp.bfloat16)
-                for at in range(inner)
-            ],
-            axis=0,
-        )
-
-        def pick(part, carry):
-            @pl.when(turn > 0)
-            def _():
-                wait_recv(blocks.at[source, part], block_recv.at[source, part])
-
-            for way, needed in forwards(source):
-
-                @pl.when(needed)
-                def _():
-                    block_copy(source, part, False, way).start()
-
-            found = jnp.dot(
-                select, blocks[source, part], preferred_element_type=jnp.float32
+        for at in range(inner):
+            select[at * capacity : (at + 1) * capacity] = jnp.where(
+                metas[source, at : at + 1, :] == slot_ids, 1.0, 0.0
             ).astype(jnp.bfloat16)
-            for at in range(inner):
-                picked[source, at, part] = found[at * capacity : (at + 1) * capacity]
-            rows[source, y, part] = picked[source, y, part]
-            for step in range(1, inner):
-                row_copy(source, step, part).start()
-            return carry
-
-        lax.fori_loop(0, parts, pick, 0)
+
+    def pick(turn, part):
+        source = source_of(turn)
+
+        @pl.when((turn == 1) | ((turn > 1) & ~needs(source)))
+        def _():
+            arrive(source, part)
+
+        @pl.when(turn == 1)
+        def _():
+            forward(source, part)
+
+        later = source_of(turn + 1)
+
+        @pl.when((turn > 0) & (turn + 1 < outer) & needs(later))
+        def _():
+            arrive(later, part)
+            forward(later, part)
+
+        found = jnp.dot(
+            select[...], blocks[source, part], preferred_element_type=jnp.float32
+        ).astype(jnp.bfloat16)
+        for at in range(inner):
+            picked[source, at, part] = found[at * capacity : (at + 1) * capacity]
+        rows[source, y, part] = picked[source, y, part]
+        for step in range(1, inner):
+            row_copy(source, step, part).start()
+
+    def apply_experts(turn):
+        source = source_of(turn)
 
         @pl.when(turn == 0)
         def _():
@@ -479,43 +495,68 @@
             for step in range(1, inner):
                 back_copy(source, step, part).start()
 
-        columns = jnp.transpose(meta)
+        columns[...] = jnp.transpose(metas[source])
         slot_lanes = lax.broadcasted_iota(jnp.int32, (tokens, capacity), 1).astype(jnp.float32)
-        spread = [
-            jnp.where(columns[:, at : at + 1] == slot_lanes, 1.0, 0.0).astype(jnp.bfloat16)
+        for at in range(inner):
+            spread[at] = jnp.where(columns[:, at : at + 1] == slot_lanes, 1.0, 0.0).astype(
+                jnp.bfloat16
+            )
+
+    def combine(turn, part):
+        source = source_of(turn)
+        for step in range(1, inner):
+            at = lax.rem(y + step, inner)
+            wait_recv(back.at[source, at, part], back_recv.at[source, at, part])
+        summed = sum(
+            jnp.dot(spread[at], back[source, at, part], preferred_element_type=jnp.float32)
+            * columns[:, inner + at : inner + at + 1]
             for at in range(inner)
-        ]
-
-        def gather_back(part, carry):
-            for step in range(1, inner):
-                at = lax.rem(y + step, inner)
-                wait_recv(back.at[source, at, part], back_recv.at[source, at, part])
-            summed = sum(
-                jnp.dot(spread[at], back[source, at, part], preferred_element_type=jnp.float32)
-                * columns[:, inner + at : inner + at + 1]
-                for at in range(inner)
-            )
-
-            @pl.when(turn == 0)
+        )
+
+        @pl.when(turn == 0)
+        def _():
+            total[part] = after_ref[part] + summed
+
+        @pl.when(turn > 0)
+        def _():
+            partial[source, part] = summed.astype(jnp.bfloat16)
+
+        for way, needed in ends(source):
+
+            @pl.when(needed)
             def _():
-                total[part] = after_ref[part] + summed
-
-            @pl.when(turn > 0)
+                sum_copy(source, part, way).start()
+
+    def turn_body(turn, carry):
+        here, before = turn < outer, turn > 0
+
+        @pl.when(here)
+        def _():
+            open_turn(turn)
+            pick(turn, 0)
+
+        @pl.when(before)
+        def _():
+            apply_experts(turn - 1)
+
+        done = 0
+        for part in range(1, parts):
+
+            @pl.when(here)
             def _():
-                partial[source, part] = summed.astype(jnp.bfloat16)
-
-            for way, needed in ends(source):
-
-                @pl.when(needed)
-                def _():
-                    sum_copy(source, part, way).start()
-
-            return carry
-
-        lax.fori_loop(0, parts, gather_back, 0)
+                pick(turn, part)
+
+            upto = parts * part // (parts - 1)
+
+            @pl.when(before)
+            def _():
+                for at in range(done, upto):
+                    combine(turn - 1, at)
+
+            done = upto
         return carry
 
-    lax.fori_loop(0, outer, turn_body, 0)
+    lax.fori_loop(0, outer + 1, turn_body, 0)
 
     def relay(tick, carry):
         for way in (-1, 1):
@@ -602,6 +643,9 @@
             pltpu.VMEM((parts, tokens, width), f32),
             pltpu.VMEM((inner * capacity, hidden), f32),
             pltpu.VMEM((inner * capacity, hidden), f32),
+            pltpu.VMEM((inner * capacity, tokens), bf16),
+            pltpu.VMEM((tokens, meta.shape[1]), f32),
+            pltpu.VMEM((inner, tokens, capacity), bf16),
             dma((3,)),
             dma((outer,)),
             dma((outer,)),

time: 297 us -> 292 us (0.983)
  Pallas kernels: 248 us -> 242 us
    pallas_call x1, Pallas kernels: 172 us -> 167 us  [run_experts(): pl.pallas_call(functools.partial(experts_kernel, outer, inner, capacity),...]
where the time goes in v2:
time: 292 us; the launch traced here: 291 us
  Pallas kernels  242 us (83%)
  waiting for transfers between devices  22.3 us (8%)
  between operations  13.5 us (5%)
  other arithmetic  7.98 us (3%)
  local copies, waits for them, and re-layouts  5.39 us (2%)
    pallas_call x1, Pallas kernels, run_experts(): pl.pallas_call(functools.partial(experts_kernel, outer, inner, capacity),...  167 us
    pallas_call x1, Pallas kernels, gather_shared(): pl.pallas_call(functools.partial(gather_kernel, outer, inner, dp_count),...  57.7 us
    all_gather x1, waiting for transfers between devices, shards(): weights = lax.all_gather(out_proj, ('sp', 'dp'), axis=0)  21.6 us
    pallas_call x1, Pallas kernels, attend(): pl.pallas_call(functools.partial(attend_kernel, heads_here, nope, channel...  9.27 us
    pallas_call x1, Pallas kernels, project(): pl.pallas_call(project_kernel, grid=(parts,), in_specs=[pl.BlockSpec((tok...  8.26 us
  transfers between devices with their start and end apart: 1, of which 1 were waited for; matrix products, arithmetic and copies ran while one was open for 4% of the time, Pallas kernels for 23%

profile of v2, /device:TPU:0, one launch (start us, length us, event | category | flops | bytes accessed | tf_op | source)
XLA Modules:
  0.0 291.2 jit_solution(14064354277170629017)
XLA Ops:
  6.5 0.0 copy-start.2
  6.5 0.0 all-gather.3.cloned.1.call-start
  6.5 0.7 all-gather.3.cloned.1.call-update
  7.3 0.1 pad.16.clone
  7.4 0.1 pad.12.clone
  7.4 0.9 copy.39
  8.4 0.6 subtract_convert_fusion.1
  8.9 0.1 copy.37
  9.0 0.1 copy.38
  9.1 1.6 copy.35
  10.7 0.7 fusion.4
  11.4 0.6 reduce-window.6
  12.0 0.2 slice_reduce_fusion
  12.3 0.1 add_add_fusion
  12.4 0.7 select_reduce_fusion
  13.1 0.6 select_maximum_fusion.meta_ref
  13.7 1.4 fusion.3.piece_ref
  15.1 0.0 copy-done.1
  15.1 0.1 fusion
  15.3 0.0 copy-done.2
  15.3 0.1 fusion.2
  15.4 0.8 maximum_maximum_fusion.row_ref
  16.2 0.0 copy-done
  16.2 0.1 bitcast_convert_fusion
  16.3 0.2 subtract_convert_fusion
  16.4 2.0 maximum_bitcast_fusion.query_ref
  18.4 57.7 %shard_map.145 = (bf16[8,256,384]{2,1,0:T(8,128)(2,1)}, bf16[4,8,64,512]{3,2,1,0:T(8,128)(2,1)}) custom-call(bf16[256,384]{1,0:T(8,128)(2,1)} %maximum_maximum_fusion.row_ref, bf16[64,512]{1,0:T(8,128)(2,1)} %fusion.3.piece_ref), custom_call_target="tpu_custom_call" | custom-call | flops 20000000000 | bytes 10000000 | tf_op jit(solution)/shard_map/pallas_call | solution.py:282
  76.2 9.3 %shard_map.146.heads_ref = bf16[256,2048]{1,0:T(8,128)(2,1)} custom-call(s32[1]{0:T(128)} %bitcast.me_ref, bf16[16,256,256]{2,1,0:T(8,128)(2,1)} %maximum_bitcast_fusion.query_ref, bf16[8,256,384]{2,1,0:T(8,128)(2,1)} %get-tuple-element.9.shared_ref, bf16[4,8,64,512]{3,2,1,0:T(8,128)(2,1)} %get-tuple-element.10.ups_ref), custom_call_target="tpu_custom_call" | custom-call | flops 21474836480 | bytes 1572864 | tf_op jit(solution)/shard_map/pallas_call | solution.py:117
  85.4 21.6 %all-gather.3.cloned.1.call-done = bf16[8192,512]{1,0:T(8,128)(2,1)} async-done(((bf16[256,512]{1,0:T(8,128)(2,1)}), bf16[8192,512]{1,0:T(8,128)(2,1)}) %all-gather.3.cloned.1.call-update) | async-done | bytes 8388624 | tf_op jit(solution)/shard_map/all_gather | solution.py:706
  107.0 8.3 %shard_map.147 = (f32[4,256,512]{2,1,0:T(8,128)}, bf16[4,256,512]{2,1,0:T(8,128)(2,1)}) custom-call(bf16[256,2048]{1,0:T(8,128)(2,1)} %shard_map.146.heads_ref, bf16[8,4,256,512]{3,2,1,0:T(8,128)(2,1)} %bitcast.22, bf16[256,2048]{1,0:T(8,128)(2,1)} %bitcast.24, f32[1,2048]{1,0:T(1,128)} %bitcast.28), custom_call_target="tpu_custom_call" | custom-call | flops 2147483648 | bytes 8388608 | tf_op jit(solution)/shard_map/pallas_call | solution.py:168
  115.3 166.7 %shard_map.148 = bf16[256,2048]{1,0:T(8,128)(2,1)} custom-call(bf16[4,256,512]{2,1,0:T(8,128)(2,1)} %get-tuple-element.11.normed_ref, f32[4,8,256]{2,1,0:T(8,128)} %select_maximum_fusion.meta_ref, f32[4,256,512]{2,1,0:T(8,128)} %get-tuple-element.12.after_ref, bf16[1,2048,1024]{2,1,0:T(8,128)(2,1)} %gate_hbm.1, bf16[1,2048,1024]{2,1,0:T(8,128)(2,1)} %up_hbm.1, ...), custom_call_target="tpu_custom_call" | custom-call | flops 12884901888 | bytes 10000000 | tf_op jit(solution)/shard_map/pallas_call | solution.py:626
  282.0 2.3 copy.42
  (15 shorter events, 0.2 us)
Async XLA Ops:
  6.5 8.6 %copy-start.1 = (bf16[1,256,256]{2,1,0:T(8,128)(2,1)S(1)}, bf16[1,256,256]{2,1,0:T(8,128)(2,1)}, u32[]{:S(2)}) copy-start(bf16[1,256,256]{2,1,0:T(8,128)(2,1)} %param.17) | copy-start | bytes 393220
  6.5 8.7 %copy-start.2 = (f32[256]{0:T(256)S(1)}, f32[256]{0:T(256)}, u32[]{:S(2)}) copy-start(f32[256]{0:T(256)} %param.20) | copy-start | bytes 3076
  6.5 9.6 %copy-start = (bf16[1,256,16,64]{1,3,2,0:T(8,128)(2,1)S(1)}, bf16[1,256,16,64]{1,3,2,0:T(8,128)(2,1)}, u32[]{:S(2)}) copy-start(bf16[1,256,16,64]{1,3,2,0:T(8,128)(2,1)} %param.16) | copy-start | bytes 1572868
  6.5 100.5 %all-gather.3.cloned.1.call-start = ((), (), s32[]{:S(2)}) async-start(), calls=%async_computation | async-start | bytes 8650752 | tf_op jit(solution)/shard_map/all_gather | solution.py:706
Sparse Core Ops, SparseCore 0:
  10.2 96.7 all-gather.2

commit v3 on v2

--- a/solution.py
+++ b/solution.py
@@ -41,264 +41,339 @@
     return floats * lax.rsqrt(jnp.mean(floats * floats, axis=-1, keepdims=True) + epsilon) * gain
 
 
-def attend_kernel(heads_here, nope, channels, scale, me_ref, query_ref, shared_ref, ups_ref, out_ref):
-    group = pl.program_id(0)
+def front_kernel(
+    outer, inner, cores, heads_here, nope, channels, scale,
+    row_ref, piece_ref, block_ref, query_ref, resid_ref, gain_ref, after_ref, normed_ref,
+    shared, ups, weights, heads, *sems,
+):
+    me, dp = lax.axis_index("sp"), lax.axis_index("dp")
+    z, y = me // inner, lax.rem(me, inner)
+    lanes = weights.shape[0] // cores
+    x, core = dp // cores, lax.rem(dp, cores)
+    groups, tokens = shared.shape[0], shared.shape[1]
     columns = heads_here * nope
-    me = me_ref[0]
-    tokens = shared_ref.shape[1]
-    ups = ups_ref[...].reshape(channels, 2 * columns)
-    up_keys = ups[:, 0:columns]
-    up_values = ups[:, columns : 2 * columns]
-    up_values_t = jnp.transpose(up_values.astype(jnp.float32)).astype(jnp.bfloat16)
-
-    def scores_of(chunk):
-        latent = shared_ref[chunk, :, 0:channels]
-        turned = shared_ref[chunk, :, channels:]
-        keys = jnp.dot(latent, up_keys, preferred_element_type=jnp.float32).astype(jnp.bfloat16)
-        values_t = lax.dot_general(
-            up_values_t, latent, (((1,), (1,)), ((), ())), preferred_element_type=jnp.float32
-        ).astype(jnp.bfloat16)
-        scores = []
-        for head in range(heads_here):
-            full = jnp.concatenate([keys[:, head * nope : (head + 1) * nope], turned], axis=1)
-            scores.append(
-                jnp.dot(full, query_ref[head], preferred_element_type=jnp.float32)
-                * (scale * log2_e)
-            )
-        return scores, [values_t[h * nope : (h + 1) * nope, :] for h in range(heads_here)]
-
-    key_ids = lax.broadcasted_iota(jnp.int32, (tokens, tokens), 0)
-    query_ids = lax.broadcasted_iota(jnp.int32, (tokens, tokens), 1)
-    allowed = key_ids <= query_ids
-    scores, values = scores_of(me)
-    state = []
-    for score, value in zip(scores, values):
-        score = jnp.where(allowed, score, masked_score)
-        largest = jnp.max(score, axis=0, keepdims=True)
-        powers = jnp.exp2(score - largest)
-        state.append(
-            (
-                largest,
-                jnp.sum(powers, axis=0, keepdims=True),
-                jnp.dot(value, powers.astype(jnp.bfloat16), preferred_element_type=jnp.float32),
-            )
+    total = groups * columns
+    row_sems, piece_sems, block_sems = sems[0:4], sems[4:12], sems[12:20]
+
+    def remote(source, target, send, recv, peer):
+        return pltpu.make_async_remote_copy(
+            src_ref=source, dst_ref=target, send_sem=send, recv_sem=recv,
+            device_id=peer, device_id_type=pl.DeviceIdType.MESH,
         )
 
-    def step(chunk, state):
-        scores, values = scores_of(chunk)
-        after = []
-        for (largest, total, kept), score, value in zip(state, scores, values):
-            now = jnp.maximum(largest, jnp.max(score, axis=0, keepdims=True))
-            fade = jnp.exp2(largest - now)
-            powers = jnp.exp2(score - now)
-            after.append(
-                (
-                    now,
-                    total * fade + jnp.sum(powers, axis=0, keepdims=True),
-                    kept * fade
-                    + jnp.dot(
-                        value, powers.astype(jnp.bfloat16), preferred_element_type=jnp.float32
-                    ),
-                )
-            )
-        return tuple(after)
-
-    state = lax.fori_loop(0, me, step, tuple(state))
-    for head, (_, total, kept) in enumerate(state):
-        out_ref[:, head * nope : (head + 1) * nope] = jnp.transpose(kept / total).astype(
-            out_ref.dtype
-        )
-
-
-def attend(me, queries_t, shared, ups, heads_here, nope, channels, scale):
-    groups, tokens, width = shared.shape
-    columns = heads_here * nope
-    depth = queries_t.shape[1]
-    return pl.pallas_call(
-        functools.partial(attend_kernel, heads_here, nope, channels, scale),
-        grid_spec=pltpu.PrefetchScalarGridSpec(
-            num_scalar_prefetch=1,
-            grid=(groups,),
-            in_specs=[
-                pl.BlockSpec((heads_here, depth, tokens), lambda g, me: (g, 0, 0)),
-                pl.BlockSpec((groups, tokens, width), lambda g, me: (0, 0, 0)),
-                pl.BlockSpec((ups.shape[0], 1) + ups.shape[2:], lambda g, me: (0, g, 0, 0)),
-            ],
-            out_specs=pl.BlockSpec((tokens, columns), lambda g, me: (0, g)),
-        ),
-        out_shape=jax.ShapeDtypeStruct((tokens, groups * columns), jnp.bfloat16),
-        cost_estimate=pl.CostEstimate(
-            flops=20 * groups * tokens * groups * tokens * columns,
-            bytes_accessed=2 * groups * tokens * width,
-            transcendentals=0,
-        ),
-    )(me, queries_t, shared, ups)
-
-
-def project_kernel(heads_ref, weight_ref, resid_ref, gain_ref, after_ref, normed_ref, square_ref):
-    part = pl.program_id(0)
-    rows, width = weight_ref.shape[0] * weight_ref.shape[2], weight_ref.shape[3]
-    weight = weight_ref[...].reshape(rows, width)
-    projected = (
-        jnp.dot(heads_ref[...], weight, preferred_element_type=jnp.float32)
-        .astype(jnp.bfloat16)
-        .astype(jnp.float32)
-    )
-    after = resid_ref[...].astype(jnp.float32) + projected
-    after_ref[part] = after
-
-    @pl.when(part == 0)
-    def _():
-        square_ref[...] = jnp.zeros_like(square_ref)
-
-    square_ref[...] += jnp.sum(after * after, axis=1, keepdims=True)
-
-    @pl.when(part == pl.num_programs(0) - 1)
-    def _():
-        parts = after_ref.shape[0]
-        factor = lax.rsqrt(square_ref[...] / (parts * width) + epsilon)
-        for at in range(parts):
-            cols = slice(at * width, (at + 1) * width)
-            normed_ref[at] = (after_ref[at] * factor * gain_ref[:, cols]).astype(normed_ref.dtype)
-
-
-def project(heads, weights, resid, gain):
-    groups, parts, rows, width = weights.shape
-    tokens = heads.shape[0]
-    return pl.pallas_call(
-        project_kernel,
-        grid=(parts,),
-        in_specs=[
-            pl.BlockSpec((tokens, groups * rows), lambda p: (0, 0)),
-            pl.BlockSpec((groups, 1, rows, width), lambda p: (0, p, 0, 0)),
-            pl.BlockSpec((tokens, width), lambda p: (0, p)),
-            pl.BlockSpec((1, parts * width), lambda p: (0, 0)),
-        ],
-        out_specs=[
-            pl.BlockSpec((parts, tokens, width), lambda p: (0, 0, 0)),
-            pl.BlockSpec((parts, tokens, width), lambda p: (0, 0, 0)),
-        ],
-        out_shape=[
-            jax.ShapeDtypeStruct((parts, tokens, width), jnp.float32),
-            jax.ShapeDtypeStruct((parts, tokens, width), jnp.bfloat16),
-        ],
-        scratch_shapes=[pltpu.VMEM((tokens, 1), jnp.float32)],
-        cost_estimate=pl.CostEstimate(
-            flops=2 * tokens * groups * rows * parts * width,
-            bytes_accessed=2 * groups * rows * parts * width,
-            transcendentals=0,
-        ),
-    )(heads, weights, resid, gain)
-
-
-def gather_kernel(
-    outer, inner, dp_count, row_ref, piece_ref, rows_ref, pieces_ref,
-    own_sems, far_send, far_recv, near_send, near_recv, dp_send, dp_recv,
-):
-    me = lax.axis_index("sp")
-    dp = lax.axis_index("dp")
-    far, near = me // inner, lax.rem(me, inner)
+    def at_z(step):
+        return {"sp": lax.rem(z + step, outer) * inner + y}
+
+    def at_y(step):
+        return {"sp": z * inner + lax.rem(y + step, inner)}
+
+    def at_x(step):
+        return {"dp": lax.rem(x + step, lanes) * cores + core}
+
+    def at_core(step):
+        return {"dp": x * cores + lax.rem(core + step, cores)}
+
     barrier = pltpu.get_barrier_semaphore()
-    fars = [lax.rem(far + step, outer) for step in range(1, outer)]
-    nears = [lax.rem(near + step, inner) for step in range(1, inner)]
-    dps = [lax.rem(dp + step, dp_count) for step in range(1, dp_count)]
     greeted = (
-        [{"sp": f * inner + near} for f in fars]
-        + [{"sp": far * inner + n} for n in nears]
-        + [{"dp": d} for d in dps]
+        [at_z(step) for step in range(1, outer)]
+        + [at_y(step) for step in range(1, inner)]
+        + [at_x(step) for step in range(1, lanes)]
+        + [at_core(step) for step in range(1, cores)]
     )
     for peer in greeted:
         pl.semaphore_signal(barrier, inc=1, device_id=peer, device_id_type=pl.DeviceIdType.MESH)
     pl.semaphore_wait(barrier, len(greeted))
 
-    def remote(source, target, send, recv, peer):
-        copy = pltpu.make_async_remote_copy(
-            src_ref=source, dst_ref=target, send_sem=send, recv_sem=recv,
-            device_id=peer, device_id_type=pl.DeviceIdType.MESH,
-        )
-        copy.start()
-        return copy
-
-    def pair(row, piece, block, send, recv, peer):
-        return [
-            remote(row, rows_ref.at[block], send.at[0], recv.at[0], peer),
-            remote(piece, pieces_ref.at[dp, block], send.at[1], recv.at[1], peer),
-        ]
-
-    out_far = []
-    for at, f in enumerate(fars):
-        out_far.append(pair(row_ref, piece_ref, me, far_send.at[at], far_recv.at[at], {"sp": f * inner + near}))
-    last = []
-
-    def share(block):
-        for at, d in enumerate(dps):
-            last.append(
-                remote(
-                    pieces_ref.at[dp, block], pieces_ref.at[dp, block],
-                    dp_send.at[len(last)], dp_recv.at[len(last)], {"dp": d},
+    def member(index):
+        along_z, along_y = lax.rem(index, outer), index // outer
+        return lax.rem(z + along_z, outer) * inner + lax.rem(y + along_y, inner)
+
+    class Spread:
+        def __init__(self, own, held, sems, wide):
+            self.own, self.held, self.sems, self.wide = own, held, sems, wide
+
+        def place(self, block, row=None):
+            return self.held.at[block] if not self.wide else self.held.at[dp if row is None else row, block]
+
+        def along_z(self, step):
+            return remote(self.own, self.place(me), self.sems[0].at[step - 1], self.sems[1].at[step - 1], at_z(step))
+
+        def along_y(self, step, index):
+            source = self.own if isinstance(index, int) and index == 0 else self.place(member(index))
+            return remote(
+                source, self.place(member(index)),
+                self.sems[2].at[step - 1, index], self.sems[3].at[step - 1, index], at_y(step),
+            )
+
+        def along_x(self, step, index):
+            source = self.own if isinstance(index, int) and index == 0 else self.place(member(index))
+            return remote(
+                source, self.place(member(index)),
+                self.sems[4].at[step - 1, index], self.sems[5].at[step - 1, index], at_x(step),
+            )
+
+        def across(self, step, lane, index):
+            row = lax.rem(x + lane, lanes) * cores + core
+            own = isinstance(index, int) and index == 0 and lane == 0
+            source = self.own if own else self.place(member(index), row)
+            return remote(
+                source, self.place(member(index), row),
+                self.sems[6].at[step - 1, lane, index], self.sems[7].at[step - 1, lane, index], at_core(step),
+            )
+
+        def wait(self, ref, sem):
+            remote(ref, ref, self.sems[0].at[0], sem, at_z(0)).wait_recv()
+
+        def start_z(self):
+            for step in range(1, outer):
+                self.along_z(step).start()
+
+        def start_y(self, index):
+            for step in range(1, inner):
+                self.along_y(step, index).start()
+
+        def start_wide(self, index):
+            for step in range(1, lanes):
+                self.along_x(step, index).start()
+            for step in range(1, cores):
+                self.across(step, 0, index).start()
+
+        def from_z(self, index):
+            step = (outer - index) % outer
+            self.wait(self.place(member(index)), self.sems[1].at[step - 1])
+
+        def from_y(self, index):
+            step = inner - index // outer
+            self.wait(self.place(member(index)), self.sems[3].at[step - 1, lax.rem(index, outer)])
+
+        def from_x(self, lane, index):
+            row = lax.rem(x + lane, lanes) * cores + core
+            self.wait(self.place(member(index), row), self.sems[5].at[lanes - lane - 1, index])
+            for step in range(1, cores):
+                self.across(step, lane, index).start()
+
+        def from_core(self, step, lane, index):
+            row = lax.rem(x + lane, lanes) * cores + lax.rem(core + step, cores)
+            self.wait(self.place(member(index), row), self.sems[7].at[cores - step - 1, lane, index])
+
+        def drain(self):
+            for step in range(1, outer):
+                self.along_z(step).wait_send()
+            for index in range(outer):
+                for step in range(1, inner):
+                    self.along_y(step, index).wait_send()
+            if self.wide:
+
+                def one(index, carry):
+                    for step in range(1, lanes):
+                        self.along_x(step, index).wait_send()
+                    for step in range(1, cores):
+                        for lane in range(lanes):
+                            self.across(step, lane, index).wait_send()
+                    return carry
+
+                lax.fori_loop(0, groups, one, 0)
+
+    row = Spread(row_ref, shared, row_sems, False)
+    piece = Spread(piece_ref, ups, piece_sems, True)
+    block = Spread(block_ref, weights, block_sems, True)
+    row.start_z()
+    piece.start_z()
+    row.start_y(0)
+    piece.start_y(0)
+    piece.start_wide(0)
+    shared[me] = row_ref[...]
+    ups[dp, me] = piece_ref[...]
+    weights[dp, me] = block_ref[...]
+    for index in range(1, outer):
+        row.from_z(index)
+        row.start_y(index)
+        piece.from_z(index)
+        piece.start_y(index)
+        piece.start_wide(index)
+    block.start_z()
+    block.start_y(0)
+    block.start_wide(0)
+    for index in range(outer, groups):
+        row.from_y(index)
+        piece.from_y(index)
+        piece.start_wide(index)
+    for lane in range(1, lanes):
+        for index in range(groups):
+            piece.from_x(lane, index)
+
+    def settle(spread):
+        def one(index, carry):
+            for lane in range(lanes):
+                for step in range(1, cores):
+                    spread.from_core(step, lane, index)
+            return carry
+
+        lax.fori_loop(0, groups, one, 0)
+
+    settle(piece)
+
+    key_ids = lax.broadcasted_iota(jnp.int32, (tokens, tokens), 0)
+    query_ids = lax.broadcasted_iota(jnp.int32, (tokens, tokens), 1)
+    allowed = key_ids <= query_ids
+
+    def attend_group(group):
+        up = ups[:, group].reshape(channels, 2 * columns)
+        up_keys = up[:, 0:columns]
+        up_values = up[:, columns : 2 * columns]
+        up_values_t = jnp.transpose(up_values.astype(jnp.float32)).astype(jnp.bfloat16)
+
+        def scores_of(chunk):
+            latent = shared[chunk, :, 0:channels]
+            turned = shared[chunk, :, channels:]
+            keys = jnp.dot(latent, up_keys, preferred_element_type=jnp.float32).astype(jnp.bfloat16)
+            values_t = lax.dot_general(
+                up_values_t, latent, (((1,), (1,)), ((), ())), preferred_element_type=jnp.float32
+            ).astype(jnp.bfloat16)
+            scores = []
+            for head in range(heads_here):
+                full = jnp.concatenate([keys[:, head * nope : (head + 1) * nope], turned], axis=1)
+                scores.append(
+                    jnp.dot(
+                        full, query_ref[group * heads_here + head], preferred_element_type=jnp.float32
+                    )
+                    * (scale * log2_e)
+                )
+            return scores, [values_t[h * nope : (h + 1) * nope, :] for h in range(heads_here)]
+
+        scores, values = scores_of(me)
+        state = []
+        for score, value in zip(scores, values):
+            score = jnp.where(allowed, score, masked_score)
+            largest = jnp.max(score, axis=0, keepdims=True)
+            powers = jnp.exp2(score - largest)
+            state.append(
+                (
+                    largest,
+                    jnp.sum(powers, axis=0, keepdims=True),
+                    jnp.dot(value, powers.astype(jnp.bfloat16), preferred_element_type=jnp.float32),
                 )
             )
 
-    sends = []
-    for at, n in enumerate(nears):
-        sends.append(pair(row_ref, piece_ref, me, near_send.at[0, at], near_recv.at[0, at], {"sp": far * inner + n}))
-    own = [
-        pltpu.make_async_copy(row_ref, rows_ref.at[me], own_sems.at[0]),
-        pltpu.make_async_copy(piece_ref, pieces_ref.at[dp, me], own_sems.at[1]),
+        def step(chunk, state):
+            scores, values = scores_of(chunk)
+            after = []
+            for (largest, total, kept), score, value in zip(state, scores, values):
+                now = jnp.maximum(largest, jnp.max(score, axis=0, keepdims=True))
+                fade = jnp.exp2(largest - now)
+                powers = jnp.exp2(score - now)
+                after.append(
+                    (
+                        now,
+                        total * fade + jnp.sum(powers, axis=0, keepdims=True),
+                        kept * fade
+                        + jnp.dot(
+                            value, powers.astype(jnp.bfloat16), preferred_element_type=jnp.float32
+                        ),
+                    )
+                )
+            return tuple(after)
+
+        state = lax.fori_loop(0, me, step, tuple(state))
+        for head, (_, total, kept) in enumerate(state):
+            start = pl.multiple_of(group * columns + head * nope, nope)
+            heads[:, pl.ds(start, nope)] = jnp.transpose(kept / total).astype(heads.dtype)
+
+    def one_group(group, carry):
+        attend_group(group)
+
+        @pl.when(group == 0)
+        def _():
+            for index in range(1, outer):
+                block.from_z(index)
+                block.start_y(index)
+                block.start_wide(index)
+
+        nearby = group + outer - 1
+
+        @pl.when((group > 0) & (nearby < groups))
+        def _():
+            block.from_y(nearby)
+            block.start_wide(nearby)
+
+        @pl.when(group >= 2)
+        def _():
+            for lane in range(1, lanes):
+                block.from_x(lane, group - 2)
+
+        return carry
+
+    lax.fori_loop(0, groups, one_group, 0)
+    for index in range(groups - 2, groups):
+        for lane in range(1, lanes):
+            block.from_x(lane, index)
+    settle(block)
+
+    parts, width = normed_ref.shape[0], normed_ref.shape[2]
+    squares = jnp.zeros((tokens, 1), jnp.float32)
+    for part in range(parts):
+        projected = (
+            jnp.dot(
+                heads[...], weights[part].reshape(total, width), preferred_element_type=jnp.float32
+            )
+            .astype(jnp.bfloat16)
+            .astype(jnp.float32)
+        )
+        cols = slice(part * width, (part + 1) * width)
+        after = resid_ref[:, cols].astype(jnp.float32) + projected
+        after_ref[part] = after
+        squares += jnp.sum(after * after, axis=1, keepdims=True)
+    factor = lax.rsqrt(squares / (parts * width) + epsilon)
+    for part in range(parts):
+        cols = slice(part * width, (part + 1) * width)
+        normed_ref[part] = (after_ref[part] * factor * gain_ref[:, cols]).astype(normed_ref.dtype)
+    row.drain()
+    piece.drain()
+    block.drain()
+
+
+def run_front(row, piece, block, queries_t, resid, gain, sp_count, dp_count, heads_here, nope, channels, scale, number):
+    outer, inner = split_of(sp_count)
+    cores = 2 if dp_count % 2 == 0 else 1
+    lanes = dp_count // cores
+    tokens, model = resid.shape
+    width = model // dp_count
+    dma = pltpu.SemaphoreType.DMA
+    narrow = [
+        dma((max(outer - 1, 1),)),
+        dma((max(outer - 1, 1),)),
+        dma((max(inner - 1, 1), outer)),
+        dma((max(inner - 1, 1), outer)),
     ]
-    for copy in own:
-        copy.start()
-    for copy in own:
-        copy.wait()
-    share(me)
-    for at in range(outer - 1):
-        for copy in out_far[at]:
-            copy.wait_recv()
-        block = lax.rem(far + outer - 1 - at, outer) * inner + near
-        for to, n in enumerate(nears):
-            sends.append(
-                pair(
-                    rows_ref.at[block], pieces_ref.at[dp, block], block,
-                    near_send.at[at + 1, to], near_recv.at[at + 1, to], {"sp": far * inner + n},
-                )
-            )
-        share(block)
-    for at in range(outer):
-        for to in range(inner - 1):
-            for copy in sends[at * (inner - 1) + to]:
-                copy.wait_recv()
-            column = lax.rem(near + inner - 1 - to, inner)
-            share(lax.rem(far + outer - at, outer) * inner + column)
-    for copies in out_far + sends:
-        for copy in copies:
-            copy.wait_send()
-    for copy in last:
-        copy.wait()
-
-
-def gather_shared(row, piece, sp_count, dp_count, number):
-    outer, inner = split_of(sp_count)
-    dma = pltpu.SemaphoreType.DMA
+    wide = narrow + [
+        dma((max(lanes - 1, 1), sp_count)),
+        dma((max(lanes - 1, 1), sp_count)),
+        dma((max(cores - 1, 1), lanes, sp_count)),
+        dma((max(cores - 1, 1), lanes, sp_count)),
+    ]
+    vmem = pl.BlockSpec(memory_space=pltpu.VMEM)
     return pl.pallas_call(
-        functools.partial(gather_kernel, outer, inner, dp_count),
+        functools.partial(front_kernel, outer, inner, cores, heads_here, nope, channels, scale),
         out_shape=[
-            jax.ShapeDtypeStruct((sp_count,) + row.shape, row.dtype),
-            jax.ShapeDtypeStruct((dp_count, sp_count) + piece.shape, piece.dtype),
+            jax.ShapeDtypeStruct((dp_count, tokens, width), jnp.float32),
+            jax.ShapeDtypeStruct((dp_count, tokens, width), jnp.bfloat16),
         ],
-        in_specs=[pl.BlockSpec(memory_space=pltpu.VMEM)] * 2,
-        out_specs=[pl.BlockSpec(memory_space=pltpu.VMEM)] * 2,
+        in_specs=[vmem] * 6,
+        out_specs=[vmem] * 2,
         scratch_shapes=[
-            dma((2,)),
-            dma((max(outer - 1, 1), 2)),
-            dma((max(outer - 1, 1), 2)),
-            dma((outer, max(inner - 1, 1), 2)),
-            dma((outer, max(inner - 1, 1), 2)),
-            dma((max(dp_count - 1, 1) * sp_count,)),
-            dma((max(dp_count - 1, 1) * sp_count,)),
-        ],
-        compiler_params=pltpu.CompilerParams(collective_id=number, has_side_effects=True),
+            pltpu.VMEM((sp_count,) + row.shape, row.dtype),
+            pltpu.VMEM((dp_count, sp_count) + piece.shape, piece.dtype),
+            pltpu.VMEM((dp_count, sp_count) + block.shape, block.dtype),
+            pltpu.VMEM((tokens, model), jnp.bfloat16),
+        ]
+        + narrow
+        + wide
+        + wide,
+        compiler_params=pltpu.CompilerParams(
+            collective_id=number, has_side_effects=True, vmem_limit_bytes=40 * 2**20
+        ),
         cost_estimate=pl.CostEstimate(flops=2 * 10**10, bytes_accessed=10**7, transcendentals=0),
-    )(row, piece)
+    )(row, piece, block, queries_t, resid, gain)
 
 
 def split_of(sp_count):
@@ -702,19 +777,16 @@
     ups = lax.dynamic_slice_in_dim(
         jnp.concatenate([key_up, value_up], axis=1), lax.axis_index("dp") * piece, piece, axis=0
     )
-    shared, ups = gather_shared(row, ups, sp_count, dp_count, 0)
-    weights = lax.all_gather(out_proj, ("sp", "dp"), axis=0)
-    weights = weights.reshape(sp_count, dp_count, *out_proj.shape)
     query_turned = rotate(query_rope[0], local_pos)
     queries = jnp.concatenate(
         [query_nope[0], query_turned, jnp.zeros(query_turned.shape[:2] + (128 - rope,), jnp.bfloat16)],
         axis=-1,
     )
     queries_t = jnp.transpose(queries, (1, 2, 0))
-    heads = attend(
-        me.astype(jnp.int32)[None], queries_t, shared, ups, heads_here, nope, channels, scale
+    after, normed = run_front(
+        row, ups, out_proj, queries_t, resid[0], norm_gain[None],
+        sp_count, dp_count, heads_here, nope, channels, scale, 0,
     )
-    after, normed = project(heads, weights, resid[0], norm_gain[None])
 
     experts_all = sp_count * expert_gate.shape[0]
     capacity = 4 * tokens // experts_all

time: 292 us -> 266 us (0.911)
  waiting for transfers between devices: 22.3 us -> 0 us
  between operations: 13.5 us -> 0.19 us
  Pallas kernels: 242 us -> 247 us
  local copies, waits for them, and re-layouts: 5.39 us -> 9.26 us
    all_gather x1 -> x0, waiting for transfers between devices: 21.6 us -> none  [shards(): weights = lax.all_gather(out_proj, ('sp', 'dp'), axis=0)]
    pallas_call x3 -> x1, Pallas kernels: 75.2 us -> 89.6 us  [run_front(): pl.pallas_call(functools.partial(front_kernel, outer, inner, cores, heads...]
    pallas_call x1, Pallas kernels: 167 us -> 157 us  [run_experts(): pl.pallas_call(functools.partial(experts_kernel, outer, inner, capacity),...]
    unnamed x9 -> x23, local copies, waits for them, and re-layouts: 4.83 us -> 8.12 us
  transfers between devices with their start and end apart: 1 -> 0, of which waited for: 1 -> 0; matrix products, arithmetic and copies ran while one was open for 4% -> 0% of each run, Pallas kernels for 23% -> 0%
where the time goes in v3:
time: 266 us; the launch traced here: 265 us
  Pallas kernels  247 us (93%)
  local copies, waits for them, and re-layouts  9.26 us (3%)
  other arithmetic  8.54 us (3%)
    pallas_call x1, Pallas kernels, run_experts(): pl.pallas_call(functools.partial(experts_kernel, outer, inner, capacity),...  157 us
    pallas_call x1, Pallas kernels, run_front(): pl.pallas_call(functools.partial(front_kernel, outer, inner, cores, heads...  89.6 us
    unnamed x23, local copies, waits for them, and re-layouts  8.12 us

profile of v3, /device:TPU:0, one launch (start us, length us, event | category | flops | bytes accessed | tf_op | source)
XLA Modules:
  0.0 265.1 jit_solution(1429946893747695282)
XLA Ops:
  0.0 1.0 copy.35
  1.0 1.2 multiply_cosine_fusion
  2.2 0.1 copy.38
  2.3 0.1 copy.39
  2.4 0.0 copy-start.9
  2.4 1.2 bitcast_convert_fusion
  3.6 0.0 copy-start
  3.6 0.0 copy-start.2
  3.6 0.8 subtract_convert_fusion
  4.5 0.7 pad.10.clone
  5.1 0.0 copy-done.5
  5.1 1.6 copy.37
  6.7 1.9 maximum_bitcast_fusion.query_ref
  8.6 0.1 pad.16.clone
  8.7 0.0 copy-done.6
  8.7 0.1 fusion
  8.8 0.1 fusion.2
  8.9 1.0 maximum_maximum_fusion.row_ref
  9.9 0.8 fusion.3.piece_ref
  10.7 0.0 copy-start.1
  10.7 0.9 copy-done.1
  11.7 89.6 %shard_map.145 = (f32[4,256,512]{2,1,0:T(8,128)S(1)}, bf16[4,256,512]{2,1,0:T(8,128)(2,1)S(1)}) custom-call(bf16[256,384]{1,0:T(8,128)(2,1)S(1)} %maximum_maximum_fusion.row_ref, bf16[64,512]{1,0:T(8,128)(2,1)S(1)} %fusion.3.piece_ref, bf16[256,512]{1,0:T(8,128)(2,1)S(1)} %copy-done.1, bf16[16,256,256]{2,1,0:T(8,128)(2,1)S(1)} %maximum_bitcast_fusion.query_ref, ...), custom_call_target="tpu_custom_call" | custom-call | flops 20000000000 | bytes 10000000 | tf_op jit(solution)/shard_map/pallas_call | solution.py:355
  101.3 0.0 copy-start.3
  101.3 1.3 copy-done.3
  102.7 1.0 copy-done.4
  103.7 0.6 reduce-window.6
  104.2 0.2 slice_reduce_fusion
  104.5 0.1 add_add_fusion
  104.6 0.0 copy-done.8
  104.7 0.6 select_maximum_fusion.meta_ref
  105.3 157.5 %shard_map.146 = bf16[256,2048]{1,0:T(8,128)(2,1)} custom-call(bf16[4,256,512]{2,1,0:T(8,128)(2,1)} %copy-done.4, f32[4,8,256]{2,1,0:T(8,128)} %select_maximum_fusion.meta_ref, f32[4,256,512]{2,1,0:T(8,128)} %copy-done.3, bf16[1,2048,1024]{2,1,0:T(8,128)(2,1)} %gate_hbm.1, bf16[1,2048,1024]{2,1,0:T(8,128)(2,1)} %up_hbm.1, bf16[1,1024,2048]{2,1,0:T(8,128)(2,1)} %down_hbm.1), custom_call_target="tpu_custom_call" | custom-call | flops 12884901888 | bytes 10000000 | tf_op jit(solution)/shard_map/pallas_call | solution.py:701
  262.8 2.3 copy.42
  (24 shorter events, 0.2 us)
Async XLA Ops:
  0.0 5.1 %copy-start.5 = (bf16[1,256,16,128]{3,2,1,0:T(8,128)(2,1)S(1)}, bf16[1,256,16,128]{3,2,1,0:T(8,128)(2,1)}, u32[]{:S(2)}) copy-start(bf16[1,256,16,128]{3,2,1,0:T(8,128)(2,1)} %param.15) | copy-start | bytes 3145732
  2.4 6.3 %copy-start.6 = (bf16[1,256,256]{2,1,0:T(8,128)(2,1)S(1)}, bf16[1,256,256]{2,1,0:T(8,128)(2,1)}, u32[]{:S(2)}) copy-start(bf16[1,256,256]{2,1,0:T(8,128)(2,1)} %param.17) | copy-start | bytes 393220
  2.4 6.4 %copy-start.9 = (f32[256]{0:T(256)S(1)}, f32[256]{0:T(256)}, u32[]{:S(2)}) copy-start(f32[256]{0:T(256)} %param.20) | copy-start | bytes 3076
  3.6 7.1 %copy-start = (bf16[1,256,2048]{2,1,0:T(8,128)(2,1)S(1)}, bf16[1,256,2048]{2,1,0:T(8,128)(2,1)}, u32[]{:S(2)}) copy-start(bf16[1,256,2048]{2,1,0:T(8,128)(2,1)} %param.19) | copy-start | bytes 3145732
  3.6 7.1 %copy-start.2 = (f32[2048]{0:T(1024)S(1)}, f32[2048]{0:T(1024)}, u32[]{:S(2)}) copy-start(f32[2048]{0:T(1024)} %param.24) | copy-start | bytes 24580
  10.7 1.0 copy-start.1
  11.7 92.0 %copy-start.7 = (s32[1,256,2]{1,2,0:T(2,128)S(1)}, s32[1,256,2]{1,2,0:T(2,128)}, u32[]{:S(2)}) copy-start(s32[1,256,2]{1,2,0:T(2,128)} %param.28) | copy-start | bytes 6148
  11.7 93.0 %copy-start.8 = (f32[1,256,2]{1,2,0:T(2,128)S(1)}, f32[1,256,2]{1,2,0:T(2,128)}, u32[]{:S(2)}) copy-start(f32[1,256,2]{1,2,0:T(2,128)} %param.29) | copy-start | bytes 6148
  101.3 1.4 copy-start.3
  102.7 1.0 copy-start.4

commit v4 on v3

--- a/solution.py
+++ b/solution.py
@@ -12,6 +12,9 @@
 rope_base = 10000.0
 masked_score = -1e30
 log2_e = 1.4426950408889634
+part_width = 256
+link_rate = 46.6e3
+link_delay = 2.2
 
 
 def rotate(values, positions):
@@ -309,7 +312,8 @@
             block.from_x(lane, index)
     settle(block)
 
-    parts, width = normed_ref.shape[0], normed_ref.shape[2]
+    parts, width = weights.shape[0], weights.shape[3]
+    pieces, narrow = normed_ref.shape[0], normed_ref.shape[2]
     squares = jnp.zeros((tokens, 1), jnp.float32)
     for part in range(parts):
         projected = (
@@ -321,11 +325,13 @@
         )
         cols = slice(part * width, (part + 1) * width)
         after = resid_ref[:, cols].astype(jnp.float32) + projected
-        after_ref[part] = after
+        each = width // narrow
+        for at in range(each):
+            after_ref[part * each + at] = after[:, at * narrow : (at + 1) * narrow]
         squares += jnp.sum(after * after, axis=1, keepdims=True)
     factor = lax.rsqrt(squares / (parts * width) + epsilon)
-    for part in range(parts):
-        cols = slice(part * width, (part + 1) * width)
+    for part in range(pieces):
+        cols = slice(part * narrow, (part + 1) * narrow)
         normed_ref[part] = (after_ref[part] * factor * gain_ref[:, cols]).astype(normed_ref.dtype)
     row.drain()
     piece.drain()
@@ -337,7 +343,7 @@
     cores = 2 if dp_count % 2 == 0 else 1
     lanes = dp_count // cores
     tokens, model = resid.shape
-    width = model // dp_count
+    width = min(model // dp_count, part_width)
     dma = pltpu.SemaphoreType.DMA
     narrow = [
         dma((max(outer - 1, 1),)),
@@ -355,8 +361,8 @@
     return pl.pallas_call(
         functools.partial(front_kernel, outer, inner, cores, heads_here, nope, channels, scale),
         out_shape=[
-            jax.ShapeDtypeStruct((dp_count, tokens, width), jnp.float32),
-            jax.ShapeDtypeStruct((dp_count, tokens, width), jnp.bfloat16),
+            jax.ShapeDtypeStruct((model // width, tokens, width), jnp.float32),
+            jax.ShapeDtypeStruct((model // width, tokens, width), jnp.bfloat16),
         ],
         in_specs=[vmem] * 6,
         out_specs=[vmem] * 2,
@@ -381,8 +387,96 @@
     return sp_count // inner, inner
 
 
+def plan_tasks(outer, parts, across_z, across_y):
+    def forward(at, source):
+        return 1 if source < at < outer - 1 else (-1 if 0 < at < source else 0)
+
+    spent = {"A": 0.5, "B": 4.5, "C": 0.6, "F": 0.05, "R": 0.3}
+    todo = [
+        [("B", s, 0) for s in range(outer)]
+        + [(kind, s, p) for s in range(outer) for p in range(parts) for kind in "AC"]
+        + [("F", s, p) for s in range(outer) for p in range(parts) if forward(at, s)]
+        + [("R", s, p) for s in range(outer) for p in range(parts) if s != at and 0 < at < outer - 1]
+        for at in range(outer)
+    ]
+    free, landed = {}, {}
+    clock, done, order = [2.0] * outer, [set() for _ in range(outer)], [[] for _ in range(outer)]
+
+    def send(at, link, target, key, time, length):
+        free[at, link] = max(time, free.get((at, link), 0.0)) + length
+        landed[target, key] = free[at, link] + link_delay
+
+    def ready(at, task):
+        kind, source, part = task
+        needed, before = [], []
+        wait = 0.0
+        if kind in "AF" and source != at:
+            needed.append(("block", source, part))
+        if kind == "A":
+            before += [("F", source, part)] if forward(at, source) else []
+            before += [("A", source, part - 1)] if part else []
+            wait = free.get((at, "y"), 0.0) - 3.0
+        if kind == "F" and part:
+            before.append(("F", source, part - 1))
+        if kind == "B":
+            before += [("A", source, p) for p in range(parts)]
+            before += [("B", s, 0) for s in range(outer) if s != at and source == at]
+            needed += [("row", source, p) for p in range(parts)]
+            wait = free.get((at, "y"), 0.0) - 6.0
+        if kind == "C":
+            before.append(("B", source, 0))
+            needed.append(("back", source, part))
+        if kind == "R":
+            before.append(("C", source, part))
+            needed.append(("sum", source, part))
+        if any(task not in done[at] for task in before) or any((at, key) not in landed for key in needed):
+            return None
+        return max([clock[at], wait] + [landed[at, key] for key in needed])
+
+    def rank(at, task):
+        kind, source, part = task
+        own = source == at
+        return (8 if own and kind == "C" else "FRBCA".index(kind), abs(source - at), part)
+
+    for at in range(outer):
+        for part in range(parts):
+            for way in (1, -1):
+                if 0 <= at + way < outer:
+                    send(at, way, at + way, ("block", at, part), 2.0, across_z)
+    while any(todo):
+        chosen = None
+        for at in range(outer):
+            times = [(ready(at, task), task) for task in todo[at]]
+            times = [(time, task) for time, task in times if time is not None]
+            if times:
+                first = min(time for time, _ in times)
+                task = min((t for time, t in times if time <= first), key=lambda t: rank(at, t))
+                if chosen is None or first < chosen[0]:
+                    chosen = (first, at, task)
+        time, at, task = chosen
+        kind, source, part = task
+        todo[at].remove(task)
+        order[at].append(task)
+        done[at].add(task)
+        clock[at] = end = time + spent[kind]
+        way = -1 if source < at else 1
+        if kind == "F":
+            send(at, forward(at, source), at + forward(at, source), ("block", source, part), end, across_z)
+        if kind == "A":
+            send(at, "y", at, ("row", source, part), end, across_y)
+        if kind == "B":
+            for p in range(parts):
+                begun = end - spent["B"] * 0.5 * (parts - 1 - p) / parts
+                send(at, "y", at, ("back", source, p), begun, across_y)
+        last = at == (outer - 1 if way < 0 else 0)
+        if source != at and (kind == "R" or (kind == "C" and last)):
+            key = ("last", at + way, part) if way > 0 and source == at + way else ("sum", source, part)
+            send(at, way, at + way, key, end, across_z)
+    return order
+
+
 def experts_kernel(
-    outer, inner, capacity,
+    outer, inner, capacity, order,
     normed_ref, meta_ref, after_ref, gate_hbm, up_hbm, down_hbm, out_ref,
     gate_w, up_w, down_w, blocks, metas, picked, rows, made, back, partial, coming, total, gate_acc, up_acc,
     select, columns, spread,
@@ -460,14 +554,39 @@
     blocks[z] = normed_ref[...]
     metas[z] = meta_ref[z]
 
-    orders = [sorted(range(outer), key=lambda s: (abs(s - at), s)) for at in range(outer)]
-
-    def source_of(turn):
-        found = jnp.int32(0)
+    kinds = "ABCFRW"
+    steps = max(len(row) for row in order) + 1
+
+    def coded(row):
+        first = [kind for kind, _, _ in row].index("B")
+        row = row[:first] + [("W", 0, 0)] + row[first:]
+        codes = [(kinds.index(kind) * outer + source) * parts + part for kind, source, part in row]
+        return codes + [len(kinds) * outer * parts] * (steps - len(codes))
+
+    base = (len(kinds) + 1) * outer * parts
+    rows_coded = [coded(row) for row in order]
+    words = []
+    for start in range(0, steps, 3):
+        value = None
         for at in range(outer):
-            for index in range(outer):
-                found = jnp.where((z == at) & (turn == index), orders[at][index], found)
-        return found
+            word = sum(code * base**index for index, code in enumerate(rows_coded[at][start : start + 3]))
+            value = jnp.int32(word) if value is None else jnp.where(z == at, word, value)
+        words.append(value)
+
+    def task_of(step):
+        index, digit = step // 3, lax.rem(step, 3)
+        level = words
+        while len(level) > 1:
+            even = lax.rem(index, 2) == 0
+            level = [
+                jnp.where(even, level[at], level[at + 1]) if at + 1 < len(level) else level[at]
+                for at in range(0, len(level), 2)
+            ]
+            index = index // 2
+        word = level[0]
+        code = jnp.where(digit == 0, word, jnp.where(digit == 1, word // base, word // base**2))
+        code = lax.rem(code, base)
+        return code // (outer * parts), lax.rem(code // parts, outer), lax.rem(code, parts)
 
     def forwards(source):
         return [
@@ -487,46 +606,25 @@
     def arrive(source, part):
         wait_recv(blocks.at[source, part], block_recv.at[source, part])
 
-    def forward(source, part):
-        for way, needed in forwards(source):
-
-            @pl.when(needed)
-            def _():
-                block_copy(source, part, False, way).start()
-
-    def open_turn(turn):
-        source = source_of(turn)
-
-        @pl.when(turn > 0)
+    def pick(source, part):
+        @pl.when((source != z) & (part == 0))
         def _():
             wait_recv(metas.at[source], meta_recv.at[source])
 
-        slot_ids = lax.broadcasted_iota(jnp.int32, (capacity, tokens), 0).astype(jnp.float32)
-        for at in range(inner):
-            select[at * capacity : (at + 1) * capacity] = jnp.where(
-                metas[source, at : at + 1, :] == slot_ids, 1.0, 0.0
-            ).astype(jnp.bfloat16)
-
-    def pick(turn, part):
-        source = source_of(turn)
-
-        @pl.when((turn == 1) | ((turn > 1) & ~needs(source)))
+        @pl.when(part == 0)
+        def _():
+            slot_ids = lax.broadcasted_iota(jnp.int32, (capacity, tokens), 0).astype(jnp.float32)
+            for at in range(inner):
+                select[source, at * capacity : (at + 1) * capacity] = jnp.where(
+                    metas[source, at : at + 1, :] == slot_ids, 1.0, 0.0
+                ).astype(jnp.bfloat16)
+
+        @pl.when((source != z) & ~needs(source))
         def _():
             arrive(source, part)
 
-        @pl.when(turn == 1)
-        def _():
-            forward(source, part)
-
-        later = source_of(turn + 1)
-
-        @pl.when((turn > 0) & (turn + 1 < outer) & needs(later))
-        def _():
-            arrive(later, part)
-            forward(later, part)
-
         found = jnp.dot(
-            select[...], blocks[source, part], preferred_element_type=jnp.float32
+            select[source], blocks[source, part], preferred_element_type=jnp.float32
         ).astype(jnp.bfloat16)
         for at in range(inner):
             picked[source, at, part] = found[at * capacity : (at + 1) * capacity]
@@ -534,28 +632,28 @@
         for step in range(1, inner):
             row_copy(source, step, part).start()
 
-    def apply_experts(turn):
-        source = source_of(turn)
-
-        @pl.when(turn == 0)
-        def _():
-            for load in loads:
-                load.wait()
-
+    def apply_experts(source):
         gate_acc[...] = jnp.zeros_like(gate_acc)
         up_acc[...] = jnp.zeros_like(up_acc)
 
-        def widen(part, carry):
-            for step in range(1, inner):
-                at = lax.rem(y + step, inner)
-                wait_recv(rows.at[source, at, part], row_recv.at[source, at, part])
-            taken = jnp.concatenate([rows[source, at, part] for at in range(inner)], axis=0)
-            depth = pl.ds(pl.multiple_of(part * width, width), width)
+        def widen(pair, carry):
+            for part in (2 * pair, 2 * pair + 1):
+                for step in range(1, inner):
+                    at = lax.rem(y + step, inner)
+                    wait_recv(rows.at[source, at, part], row_recv.at[source, at, part])
+            taken = jnp.concatenate(
+                [
+                    jnp.concatenate([rows[source, at, 2 * pair + half] for half in range(2)], axis=1)
+                    for at in range(inner)
+                ],
+                axis=0,
+            )
+            depth = pl.ds(pl.multiple_of(pair * 2 * width, 2 * width), 2 * width)
             gate_acc[...] += jnp.dot(taken, gate_w[depth, :], preferred_element_type=jnp.float32)
             up_acc[...] += jnp.dot(taken, up_w[depth, :], preferred_element_type=jnp.float32)
             return carry
 
-        lax.fori_loop(0, parts, widen, 0)
+        lax.fori_loop(0, parts // 2, widen, 0)
         gate = gate_acc[...]
         hidden = (gate / (1.0 + jnp.exp(-gate)) * up_acc[...]).astype(jnp.bfloat16)
 
@@ -570,29 +668,28 @@
             for step in range(1, inner):
                 back_copy(source, step, part).start()
 
-        columns[...] = jnp.transpose(metas[source])
+        columns[source] = jnp.transpose(metas[source])
         slot_lanes = lax.broadcasted_iota(jnp.int32, (tokens, capacity), 1).astype(jnp.float32)
         for at in range(inner):
-            spread[at] = jnp.where(columns[:, at : at + 1] == slot_lanes, 1.0, 0.0).astype(
-                jnp.bfloat16
-            )
-
-    def combine(turn, part):
-        source = source_of(turn)
+            spread[source, at] = jnp.where(
+                columns[source, :, at : at + 1] == slot_lanes, 1.0, 0.0
+            ).astype(jnp.bfloat16)
+
+    def combine(source, part):
         for step in range(1, inner):
             at = lax.rem(y + step, inner)
             wait_recv(back.at[source, at, part], back_recv.at[source, at, part])
         summed = sum(
-            jnp.dot(spread[at], back[source, at, part], preferred_element_type=jnp.float32)
-            * columns[:, inner + at : inner + at + 1]
+            jnp.dot(spread[source, at], back[source, at, part], preferred_element_type=jnp.float32)
+            * columns[source, :, inner + at : inner + at + 1]
             for at in range(inner)
         )
 
-        @pl.when(turn == 0)
+        @pl.when(source == z)
         def _():
             total[part] = after_ref[part] + summed
 
-        @pl.when(turn > 0)
+        @pl.when(source != z)
         def _():
             partial[source, part] = summed.astype(jnp.bfloat16)
 
@@ -602,58 +699,53 @@
             def _():
                 sum_copy(source, part, way).start()
 
-    def turn_body(turn, carry):
-        here, before = turn < outer, turn > 0
-
-        @pl.when(here)
-        def _():
-            open_turn(turn)
-            pick(turn, 0)
-
-        @pl.when(before)
-        def _():
-            apply_experts(turn - 1)
-
-        done = 0
-        for part in range(1, parts):
-
-            @pl.when(here)
+    def relay(source, part):
+        wait_recv(coming.at[source, part], sum_recv.at[source, part])
+        partial[source, part] = (
+            partial[source, part].astype(jnp.float32) + coming[source, part].astype(jnp.float32)
+        ).astype(jnp.bfloat16)
+        for way in (1, -1):
+
+            @pl.when((source > z) if way > 0 else (source < z))
             def _():
-                pick(turn, part)
-
-            upto = parts * part // (parts - 1)
-
-            @pl.when(before)
-            def _():
-                for at in range(done, upto):
-                    combine(turn - 1, at)
-
-            done = upto
+                sum_copy(source, part, way).start()
+
+    def run_task(step, carry):
+        kind, source, part = task_of(step)
+
+        @pl.when(kind == 0)
+        def _():
+            pick(source, part)
+
+        @pl.when(kind == 1)
+        def _():
+            apply_experts(source)
+
+        @pl.when(kind == 2)
+        def _():
+            combine(source, part)
+
+        @pl.when(kind == 3)
+        def _():
+            arrive(source, part)
+            for way, needed in forwards(source):
+
+                @pl.when(needed)
+                def _():
+                    block_copy(source, part, False, way).start()
+
+        @pl.when(kind == 4)
+        def _():
+            relay(source, part)
+
+        @pl.when(kind == 5)
+        def _():
+            for load in loads:
+                load.wait()
+
         return carry
 
-    lax.fori_loop(0, outer + 1, turn_body, 0)
-
-    def relay(tick, carry):
-        for way in (-1, 1):
-            since = tick - (z if way > 0 else outer - 1 - z)
-            part = lax.rem(since + parts * outer, parts)
-            steps = (since + parts * outer) // parts - outer
-            source = steps if way > 0 else outer - 1 - steps
-            passing = (source > z) if way > 0 else (source < z)
-            valid = (source >= 0) & (source < outer) & passing & (z - way >= 0) & (z - way < outer)
-
-            @pl.when(valid)
-            def _():
-                wait_recv(coming.at[source, part], sum_recv.at[source, part])
-                partial[source, part] = (
-                    partial[source, part].astype(jnp.float32)
-                    + coming[source, part].astype(jnp.float32)
-                ).astype(jnp.bfloat16)
-                sum_copy(source, part, way).start()
-
-        return carry
-
-    lax.fori_loop(0, outer * (parts + 1), relay, 0)
+    lax.fori_loop(0, steps, run_task, 0)
 
     for part in range(parts):
         for slot, valid in ((z, z < outer - 1), (outer, z > 0)):
@@ -693,13 +785,15 @@
     outer, inner = split_of(sp_count)
     parts, tokens, width = normed.shape
     model, hidden = gate.shape[1:]
+    across_z = tokens * width * 2 / link_rate
+    order = plan_tasks(outer, parts, across_z, across_z * capacity / tokens)
     dma = pltpu.SemaphoreType.DMA
     bf16, f32 = jnp.bfloat16, jnp.float32
     steps_y = max(inner - 1, 1)
     vmem = pl.BlockSpec(memory_space=pltpu.VMEM)
     anywhere = pl.BlockSpec(memory_space=pl.ANY)
     return pl.pallas_call(
-        functools.partial(experts_kernel, outer, inner, capacity),
+        functools.partial(experts_kernel, outer, inner, capacity, order),
         out_shape=jax.ShapeDtypeStruct((tokens, parts * width), bf16),
         in_specs=[vmem, vmem, vmem, anywhere, anywhere, anywhere],
         out_specs=vmem,
@@ -718,9 +812,9 @@
             pltpu.VMEM((parts, tokens, width), f32),
             pltpu.VMEM((inner * capacity, hidden), f32),
             pltpu.VMEM((inner * capacity, hidden), f32),
-            pltpu.VMEM((inner * capacity, tokens), bf16),
-            pltpu.VMEM((tokens, meta.shape[1]), f32),
-            pltpu.VMEM((inner, tokens, capacity), bf16),
+            pltpu.VMEM((outer, inner * capacity, tokens), bf16),
+            pltpu.VMEM((outer, tokens, meta.shape[1]), f32),
+            pltpu.VMEM((outer, inner, tokens, capacity), bf16),
             dma((3,)),
             dma((outer,)),
             dma((outer,)),

time: 266 us -> 245 us (0.921)
  Pallas kernels: 247 us -> 226 us
    pallas_call x1, Pallas kernels: 157 us -> 137 us  [run_experts(): pl.pallas_call(functools.partial(experts_kernel, outer, inner, capacity,...]
where the time goes in v4:
time: 245 us; the launch traced here: 244 us
  Pallas kernels  226 us (92%)
  local copies, waits for them, and re-layouts  9.26 us (4%)
  other arithmetic  8.54 us (3%)
    pallas_call x1, Pallas kernels, run_experts(): pl.pallas_call(functools.partial(experts_kernel, outer, inner, capacity,...  137 us
    pallas_call x1, Pallas kernels, run_front(): pl.pallas_call(functools.partial(front_kernel, outer, inner, cores, heads...  89.6 us
    unnamed x23, local copies, waits for them, and re-layouts  8.12 us

profile of v4, /device:TPU:0, one launch (start us, length us, event | category | flops | bytes accessed | tf_op | source)
XLA Modules:
  0.0 244.1 jit_solution(3070918477672014878)
XLA Ops:
  0.0 1.0 copy.35
  1.0 1.2 multiply_cosine_fusion
  2.2 0.1 copy.38
  2.3 0.1 copy.39
  2.4 0.0 copy-start.9
  2.4 1.2 bitcast_convert_fusion
  3.6 0.0 copy-start
  3.6 0.0 copy-start.2
  3.6 0.8 subtract_convert_fusion
  4.5 0.7 pad.10.clone
  5.1 0.0 copy-done.5
  5.1 1.6 copy.37
  6.7 1.9 maximum_bitcast_fusion.query_ref
  8.6 0.1 pad.16.clone
  8.7 0.0 copy-done.6
  8.7 0.1 fusion
  8.8 0.1 fusion.2
  8.9 1.0 maximum_maximum_fusion.row_ref
  9.9 0.8 fusion.3.piece_ref
  10.7 0.0 copy-done.2
  10.7 0.0 copy-start.1
  10.7 0.9 copy-done.1
  11.7 89.6 %shard_map.145 = (f32[8,256,256]{2,1,0:T(8,128)S(1)}, bf16[8,256,256]{2,1,0:T(8,128)(2,1)S(1)}) custom-call(bf16[256,384]{1,0:T(8,128)(2,1)S(1)} %maximum_maximum_fusion.row_ref, bf16[64,512]{1,0:T(8,128)(2,1)S(1)} %fusion.3.piece_ref, bf16[256,512]{1,0:T(8,128)(2,1)S(1)} %copy-done.1, bf16[16,256,256]{2,1,0:T(8,128)(2,1)S(1)} %maximum_bitcast_fusion.query_ref, ...), custom_call_target="tpu_custom_call" | custom-call | flops 20000000000 | bytes 10000000 | tf_op jit(solution)/shard_map/pallas_call | solution.py:361
  101.3 0.0 copy-start.3
  101.3 1.3 copy-done.3
  102.7 1.0 copy-done.4
  103.7 0.6 reduce-window.6
  104.2 0.2 slice_reduce_fusion
  104.5 0.1 add_add_fusion
  104.7 0.6 select_maximum_fusion.meta_ref
  105.3 136.5 %shard_map.146 = bf16[256,2048]{1,0:T(8,128)(2,1)} custom-call(bf16[8,256,256]{2,1,0:T(8,128)(2,1)} %copy-done.4, f32[4,8,256]{2,1,0:T(8,128)} %select_maximum_fusion.meta_ref, f32[8,256,256]{2,1,0:T(8,128)} %copy-done.3, bf16[1,2048,1024]{2,1,0:T(8,128)(2,1)} %gate_hbm.1, bf16[1,2048,1024]{2,1,0:T(8,128)(2,1)} %up_hbm.1, bf16[1,1024,2048]{2,1,0:T(8,128)(2,1)} %down_hbm.1), custom_call_target="tpu_custom_call" | custom-call | flops 12884901888 | bytes 10000000 | tf_op jit(solution)/shard_map/pallas_call | solution.py:795
  241.8 2.3 copy.42
  (24 shorter events, 0.2 us)
Async XLA Ops:
  0.0 5.1 %copy-start.5 = (bf16[1,256,16,128]{3,2,1,0:T(8,128)(2,1)S(1)}, bf16[1,256,16,128]{3,2,1,0:T(8,128)(2,1)}, u32[]{:S(2)}) copy-start(bf16[1,256,16,128]{3,2,1,0:T(8,128)(2,1)} %param.15) | copy-start | bytes 3145732
  2.4 6.3 %copy-start.6 = (bf16[1,256,256]{2,1,0:T(8,128)(2,1)S(1)}, bf16[1,256,256]{2,1,0:T(8,128)(2,1)}, u32[]{:S(2)}) copy-start(bf16[1,256,256]{2,1,0:T(8,128)(2,1)} %param.17) | copy-start | bytes 393220
  2.4 6.4 %copy-start.9 = (f32[256]{0:T(256)S(1)}, f32[256]{0:T(256)}, u32[]{:S(2)}) copy-start(f32[256]{0:T(256)} %param.20) | copy-start | bytes 3076
  3.6 7.1 %copy-start = (bf16[1,256,2048]{2,1,0:T(8,128)(2,1)S(1)}, bf16[1,256,2048]{2,1,0:T(8,128)(2,1)}, u32[]{:S(2)}) copy-start(bf16[1,256,2048]{2,1,0:T(8,128)(2,1)} %param.19) | copy-start | bytes 3145732
  3.6 7.1 %copy-start.2 = (f32[2048]{0:T(1024)S(1)}, f32[2048]{0:T(1024)}, u32[]{:S(2)}) copy-start(f32[2048]{0:T(1024)} %param.24) | copy-start | bytes 24580
  10.7 1.0 copy-start.1
  11.7 92.0 %copy-start.7 = (s32[1,256,2]{1,2,0:T(2,128)S(1)}, s32[1,256,2]{1,2,0:T(2,128)}, u32[]{:S(2)}) copy-start(s32[1,256,2]{1,2,0:T(2,128)} %param.28) | copy-start | bytes 6148
  11.7 93.0 %copy-start.8 = (f32[1,256,2]{1,2,0:T(2,128)S(1)}, f32[1,256,2]{1,2,0:T(2,128)}, u32[]{:S(2)}) copy-start(f32[1,256,2]{1,2,0:T(2,128)} %param.29) | copy-start | bytes 6148
  101.3 1.4 copy-start.3
  102.7 1.0 copy-start.4

commit v5 on v4

--- a/solution.py
+++ b/solution.py
@@ -46,8 +46,8 @@
 
 def front_kernel(
     outer, inner, cores, heads_here, nope, channels, scale,
-    row_ref, piece_ref, block_ref, query_ref, resid_ref, gain_ref, after_ref, normed_ref,
-    shared, ups, weights, heads, *sems,
+    row_ref, piece_ref, block_ref, nope_ref, rope_ref, cosine_ref, sine_ref, resid_ref, gain_ref,
+    after_ref, normed_ref, shared, ups, weights, heads, queries, *sems,
 ):
     me, dp = lax.axis_index("sp"), lax.axis_index("dp")
     z, y = me // inner, lax.rem(me, inner)
@@ -56,7 +56,7 @@
     groups, tokens = shared.shape[0], shared.shape[1]
     columns = heads_here * nope
     total = groups * columns
-    row_sems, piece_sems, block_sems = sems[0:4], sems[4:12], sems[12:20]
+    row_sems, piece_sems, block_sems = sems[0:4], sems[4:10], sems[10:18]
 
     def remote(source, target, send, recv, peer):
         return pltpu.make_async_remote_copy(
@@ -78,143 +78,193 @@
 
     barrier = pltpu.get_barrier_semaphore()
     greeted = (
-        [at_z(step) for step in range(1, outer)]
-        + [at_y(step) for step in range(1, inner)]
+        [at_y(step) for step in range(1, inner)]
         + [at_x(step) for step in range(1, lanes)]
         + [at_core(step) for step in range(1, cores)]
     )
+    below, above = z > 0, z < outer - 1
     for peer in greeted:
         pl.semaphore_signal(barrier, inc=1, device_id=peer, device_id_type=pl.DeviceIdType.MESH)
-    pl.semaphore_wait(barrier, len(greeted))
+    for way, there in ((-1, below), (1, above)):
+
+        @pl.when(there)
+        def _():
+            pl.semaphore_signal(
+                barrier, inc=1, device_id=at_z(way), device_id_type=pl.DeviceIdType.MESH
+            )
+
+    pl.semaphore_wait(barrier, len(greeted) + jnp.where(below & above, 2, 1 if outer > 1 else 0))
+
+    orders = [sorted(range(outer), key=lambda s: (abs(s - at), s)) for at in range(outer)]
+
+    def source_of(turn):
+        found = z
+        for index in range(1, outer):
+            value = jnp.int32(orders[0][index])
+            for at in range(1, outer):
+                value = jnp.where(z == at, orders[at][index], value)
+            found = jnp.where(turn == index, value, found)
+        return found
 
     def member(index):
-        along_z, along_y = lax.rem(index, outer), index // outer
-        return lax.rem(z + along_z, outer) * inner + lax.rem(y + along_y, inner)
+        return source_of(lax.rem(index, outer)) * inner + lax.rem(y + index // outer, inner)
 
     class Spread:
-        def __init__(self, own, held, sems, wide):
-            self.own, self.held, self.sems, self.wide = own, held, sems, wide
-
-        def place(self, block, row=None):
-            return self.held.at[block] if not self.wide else self.held.at[dp if row is None else row, block]
-
-        def along_z(self, step):
-            return remote(self.own, self.place(me), self.sems[0].at[step - 1], self.sems[1].at[step - 1], at_z(step))
-
-        def along_y(self, step, index):
-            source = self.own if isinstance(index, int) and index == 0 else self.place(member(index))
+        def __init__(self, own, held, sems, lanes, row):
+            self.own, self.held, self.sems, self.lanes, self.row = own, held, sems, lanes, row
+
+        def place(self, block, lane=0, at_core=None):
+            if self.row is None:
+                return self.held.at[block]
+            return self.held.at[self.row(lane, core if at_core is None else at_core), block]
+
+        def source(self, index, lane=0):
+            own = isinstance(index, int) and index == 0 and isinstance(lane, int) and lane == 0
+            return self.own if own else self.place(member(index), lane)
+
+        def along_z(self, turn, way):
+            block, at = member(turn), source_of(turn)
             return remote(
-                source, self.place(member(index)),
-                self.sems[2].at[step - 1, index], self.sems[3].at[step - 1, index], at_y(step),
+                self.source(turn), self.place(block),
+                self.sems[0].at[(way + 1) // 2, at], self.sems[1].at[at], at_z(way),
             )
 
+        def along_y(self, step, turn):
+            return remote(
+                self.source(turn), self.place(member(turn)),
+                self.sems[2].at[step - 1, turn], self.sems[3].at[step - 1, turn], at_y(step),
+            )
+
         def along_x(self, step, index):
-            source = self.own if isinstance(index, int) and index == 0 else self.place(member(index))
             return remote(
-                source, self.place(member(index)),
+                self.source(index), self.place(member(index)),
                 self.sems[4].at[step - 1, index], self.sems[5].at[step - 1, index], at_x(step),
             )
 
         def across(self, step, lane, index):
-            row = lax.rem(x + lane, lanes) * cores + core
-            own = isinstance(index, int) and index == 0 and lane == 0
-            source = self.own if own else self.place(member(index), row)
             return remote(
-                source, self.place(member(index), row),
-                self.sems[6].at[step - 1, lane, index], self.sems[7].at[step - 1, lane, index], at_core(step),
+                self.source(index, lane), self.place(member(index), lane),
+                self.sems[-2].at[step - 1, lane, index], self.sems[-1].at[step - 1, lane, index], at_core(step),
             )
 
         def wait(self, ref, sem):
-            remote(ref, ref, self.sems[0].at[0], sem, at_z(0)).wait_recv()
-
-        def start_z(self):
-            for step in range(1, outer):
-                self.along_z(step).start()
-
-        def start_y(self, index):
+            remote(ref, ref, self.sems[0].at[0, 0], sem, at_core(0)).wait_recv()
+
+        def start_z(self, turn):
+            at = source_of(turn)
+            for way, there in ((-1, below & (at >= z)), (1, above & (at <= z))):
+
+                @pl.when(there)
+                def _():
+                    self.along_z(turn, way).start()
+
+        def start_y(self, turn):
             for step in range(1, inner):
-                self.along_y(step, index).start()
+                self.along_y(step, turn).start()
 
         def start_wide(self, index):
-            for step in range(1, lanes):
+            if self.row is None:
+                return
+            for step in range(1, self.lanes):
                 self.along_x(step, index).start()
             for step in range(1, cores):
                 self.across(step, 0, index).start()
 
-        def from_z(self, index):
-            step = (outer - index) % outer
-            self.wait(self.place(member(index)), self.sems[1].at[step - 1])
+        def from_z(self, turn):
+            self.wait(self.place(member(turn)), self.sems[1].at[source_of(turn)])
+            self.start_z(turn)
+            self.start_y(turn)
+            self.start_wide(turn)
 
         def from_y(self, index):
             step = inner - index // outer
             self.wait(self.place(member(index)), self.sems[3].at[step - 1, lax.rem(index, outer)])
+            self.start_wide(index)
 
         def from_x(self, lane, index):
-            row = lax.rem(x + lane, lanes) * cores + core
-            self.wait(self.place(member(index), row), self.sems[5].at[lanes - lane - 1, index])
+            self.wait(self.place(member(index), lane), self.sems[5].at[self.lanes - lane - 1, index])
             for step in range(1, cores):
                 self.across(step, lane, index).start()
 
-        def from_core(self, step, lane, index):
-            row = lax.rem(x + lane, lanes) * cores + lax.rem(core + step, cores)
-            self.wait(self.place(member(index), row), self.sems[7].at[cores - step - 1, lane, index])
+        def settle(self):
+            def one(index, carry):
+                for lane in range(self.lanes):
+                    for step in range(1, cores):
+                        self.wait(
+                            self.place(member(index), lane, lax.rem(core + step, cores)),
+                            self.sems[-1].at[cores - step - 1, lane, index],
+                        )
+                return carry
+
+            lax.fori_loop(0, groups, one, 0)
 
         def drain(self):
-            for step in range(1, outer):
-                self.along_z(step).wait_send()
-            for index in range(outer):
+            for turn in range(outer):
+                at = source_of(turn)
+                for way, there in ((-1, below & (at >= z)), (1, above & (at <= z))):
+
+                    @pl.when(there)
+                    def _():
+                        self.along_z(turn, way).wait_send()
+
                 for step in range(1, inner):
-                    self.along_y(step, index).wait_send()
-            if self.wide:
-
-                def one(index, carry):
-                    for step in range(1, lanes):
-                        self.along_x(step, index).wait_send()
-                    for step in range(1, cores):
-                        for lane in range(lanes):
-                            self.across(step, lane, index).wait_send()
-                    return carry
-
-                lax.fori_loop(0, groups, one, 0)
-
-    row = Spread(row_ref, shared, row_sems, False)
-    piece = Spread(piece_ref, ups, piece_sems, True)
-    block = Spread(block_ref, weights, block_sems, True)
-    row.start_z()
-    piece.start_z()
-    row.start_y(0)
-    piece.start_y(0)
-    piece.start_wide(0)
+                    self.along_y(step, turn).wait_send()
+            if self.row is None:
+                return
+
+            def one(index, carry):
+                for step in range(1, self.lanes):
+                    self.along_x(step, index).wait_send()
+                for step in range(1, cores):
+                    for lane in range(self.lanes):
+                        self.across(step, lane, index).wait_send()
+                return carry
+
+            lax.fori_loop(0, groups, one, 0)
+
+    row = Spread(row_ref, shared, row_sems, 1, None)
+    piece = Spread(piece_ref, ups, piece_sems, 1, lambda lane, at: at)
+    block = Spread(
+        block_ref, weights, block_sems, lanes, lambda lane, at: lax.rem(x + lane, lanes) * cores + at
+    )
+    for spread in (row, piece):
+        spread.start_z(0)
+        spread.start_y(0)
+        spread.start_wide(0)
+    block.start_z(0)
+    block.start_wide(0)
     shared[me] = row_ref[...]
-    ups[dp, me] = piece_ref[...]
+    ups[core, me] = piece_ref[...]
     weights[dp, me] = block_ref[...]
-    for index in range(1, outer):
-        row.from_z(index)
-        row.start_y(index)
-        piece.from_z(index)
-        piece.start_y(index)
-        piece.start_wide(index)
-    block.start_z()
+
+    rope = cosine_ref.shape[0]
+    for pair in range(queries.shape[0] // 2):
+        both = jnp.transpose(rope_ref[:, pair * 4 * rope : (pair + 1) * 4 * rope].astype(jnp.float32))
+        for half in range(2):
+            head = 2 * pair + half
+            first = both[half * 2 * rope : half * 2 * rope + rope]
+            second = both[half * 2 * rope + rope : (half + 1) * 2 * rope]
+            cosine, sine_part = cosine_ref[...], sine_ref[...]
+            queries[head, nope : nope + 2 * rope] = jnp.concatenate(
+                [first * cosine - second * sine_part, second * cosine + first * sine_part], axis=0
+            ).astype(queries.dtype)
+            queries[head, nope + 2 * rope :] = jnp.zeros(
+                (queries.shape[1] - nope - 2 * rope, tokens), queries.dtype
+            )
+            queries[head, 0:nope] = jnp.transpose(
+                nope_ref[:, head * nope : (head + 1) * nope].astype(jnp.float32)
+            ).astype(queries.dtype)
+
+    for turn in range(1, outer):
+        row.from_z(turn)
+        piece.from_z(turn)
     block.start_y(0)
-    block.start_wide(0)
+    for turn in range(1, outer - 1):
+        block.from_z(turn)
     for index in range(outer, groups):
         row.from_y(index)
         piece.from_y(index)
-        piece.start_wide(index)
-    for lane in range(1, lanes):
-        for index in range(groups):
-            piece.from_x(lane, index)
-
-    def settle(spread):
-        def one(index, carry):
-            for lane in range(lanes):
-                for step in range(1, cores):
-                    spread.from_core(step, lane, index)
-            return carry
-
-        lax.fori_loop(0, groups, one, 0)
-
-    settle(piece)
+    piece.settle()
 
     key_ids = lax.broadcasted_iota(jnp.int32, (tokens, tokens), 0)
     query_ids = lax.broadcasted_iota(jnp.int32, (tokens, tokens), 1)
@@ -238,7 +288,7 @@
                 full = jnp.concatenate([keys[:, head * nope : (head + 1) * nope], turned], axis=1)
                 scores.append(
                     jnp.dot(
-                        full, query_ref[group * heads_here + head], preferred_element_type=jnp.float32
+                        full, queries[group * heads_here + head], preferred_element_type=jnp.float32
                     )
                     * (scale * log2_e)
                 )
@@ -287,30 +337,25 @@
 
         @pl.when(group == 0)
         def _():
-            for index in range(1, outer):
-                block.from_z(index)
-                block.start_y(index)
-                block.start_wide(index)
+            block.from_z(outer - 1)
 
         nearby = group + outer - 1
 
         @pl.when((group > 0) & (nearby < groups))
         def _():
             block.from_y(nearby)
-            block.start_wide(nearby)
-
-        @pl.when(group >= 2)
+
+        @pl.when(group >= 1)
         def _():
             for lane in range(1, lanes):
-                block.from_x(lane, group - 2)
+                block.from_x(lane, group - 1)
 
         return carry
 
     lax.fori_loop(0, groups, one_group, 0)
-    for index in range(groups - 2, groups):
-        for lane in range(1, lanes):
-            block.from_x(lane, index)
-    settle(block)
+    for lane in range(1, lanes):
+        block.from_x(lane, groups - 1)
+    block.settle()
 
     parts, width = weights.shape[0], weights.shape[3]
     pieces, narrow = normed_ref.shape[0], normed_ref.shape[2]
@@ -338,25 +383,26 @@
     block.drain()
 
 
-def run_front(row, piece, block, queries_t, resid, gain, sp_count, dp_count, heads_here, nope, channels, scale, number):
+def run_front(
+    row, piece, block, query_nope, query_rope, cosine, sine_part, resid, gain,
+    sp_count, dp_count, cores, heads_here, nope, channels, scale, number,
+):
     outer, inner = split_of(sp_count)
-    cores = 2 if dp_count % 2 == 0 else 1
     lanes = dp_count // cores
     tokens, model = resid.shape
     width = min(model // dp_count, part_width)
     dma = pltpu.SemaphoreType.DMA
     narrow = [
-        dma((max(outer - 1, 1),)),
-        dma((max(outer - 1, 1),)),
+        dma((2, outer)),
+        dma((outer,)),
         dma((max(inner - 1, 1), outer)),
         dma((max(inner - 1, 1), outer)),
     ]
-    wide = narrow + [
-        dma((max(lanes - 1, 1), sp_count)),
-        dma((max(lanes - 1, 1), sp_count)),
-        dma((max(cores - 1, 1), lanes, sp_count)),
-        dma((max(cores - 1, 1), lanes, sp_count)),
-    ]
+    beside = [dma((max(lanes - 1, 1), sp_count))] * 2
+
+    def crossing(count):
+        return [dma((max(cores - 1, 1), count, sp_count))] * 2
+
     vmem = pl.BlockSpec(memory_space=pltpu.VMEM)
     return pl.pallas_call(
         functools.partial(front_kernel, outer, inner, cores, heads_here, nope, channels, scale),
@@ -364,22 +410,26 @@
             jax.ShapeDtypeStruct((model // width, tokens, width), jnp.float32),
             jax.ShapeDtypeStruct((model // width, tokens, width), jnp.bfloat16),
         ],
-        in_specs=[vmem] * 6,
+        in_specs=[vmem] * 9,
         out_specs=[vmem] * 2,
         scratch_shapes=[
             pltpu.VMEM((sp_count,) + row.shape, row.dtype),
-            pltpu.VMEM((dp_count, sp_count) + piece.shape, piece.dtype),
+            pltpu.VMEM((cores, sp_count) + piece.shape, piece.dtype),
             pltpu.VMEM((dp_count, sp_count) + block.shape, block.dtype),
             pltpu.VMEM((tokens, model), jnp.bfloat16),
+            pltpu.VMEM((sp_count * heads_here, nope + 128, tokens), jnp.bfloat16),
         ]
         + narrow
-        + wide
-        + wide,
+        + narrow
+        + crossing(1)
+        + narrow
+        + beside
+        + crossing(lanes),
         compiler_params=pltpu.CompilerParams(
             collective_id=number, has_side_effects=True, vmem_limit_bytes=40 * 2**20
         ),
         cost_estimate=pl.CostEstimate(flops=2 * 10**10, bytes_accessed=10**7, transcendentals=0),
-    )(row, piece, block, queries_t, resid, gain)
+    )(row, piece, block, query_nope, query_rope, cosine, sine_part, resid, gain)
 
 
 def split_of(sp_count):
@@ -867,19 +917,18 @@
     row = jnp.concatenate(
         [latent_normed, key_turned, jnp.zeros((tokens, spare), jnp.bfloat16)], axis=1
     )
-    piece = channels // dp_count
+    cores = 2 if dp_count % 2 == 0 else 1
+    piece = channels // cores
     ups = lax.dynamic_slice_in_dim(
-        jnp.concatenate([key_up, value_up], axis=1), lax.axis_index("dp") * piece, piece, axis=0
+        jnp.concatenate([key_up, value_up], axis=1),
+        lax.rem(lax.axis_index("dp"), cores) * piece, piece, axis=0,
     )
-    query_turned = rotate(query_rope[0], local_pos)
-    queries = jnp.concatenate(
-        [query_nope[0], query_turned, jnp.zeros(query_turned.shape[:2] + (128 - rope,), jnp.bfloat16)],
-        axis=-1,
-    )
-    queries_t = jnp.transpose(queries, (1, 2, 0))
+    frequency = rope_base ** (-jnp.arange(rope // 2, dtype=jnp.float32) / (rope // 2))
+    angles = frequency[:, None] * local_pos.astype(jnp.float32)[None, :]
     after, normed = run_front(
-        row, ups, out_proj, queries_t, resid[0], norm_gain[None],
-        sp_count, dp_count, heads_here, nope, channels, scale, 0,
+        row, ups, out_proj, query_nope[0].reshape(tokens, -1), query_rope[0].reshape(tokens, -1),
+        jnp.cos(angles), jnp.sin(angles), resid[0], norm_gain[None],
+        sp_count, dp_count, cores, heads_here, nope, channels, scale, 0,
     )
 
     experts_all = sp_count * expert_gate.shape[0]

time: 245 us -> 230 us (0.939)
  Pallas kernels: 226 us -> 216 us
  other arithmetic: 8.54 us -> 5.25 us
    pallas_call x1, Pallas kernels: 89.6 us -> 80.5 us  [run_front(): pl.pallas_call(functools.partial(front_kernel, outer, inner, cores, heads...]
    unnamed x23 -> x17, local copies, waits for them, and re-layouts: 8.12 us -> 7.01 us
where the time goes in v5:
time: 230 us
  Pallas kernels  216 us (94%)
  local copies, waits for them, and re-layouts  8.61 us (4%)
  other arithmetic  5.25 us (2%)
    pallas_call x1, Pallas kernels, run_experts(): pl.pallas_call(functools.partial(experts_kernel, outer, inner, capacity,...  135 us
    pallas_call x1, Pallas kernels, run_front(): pl.pallas_call(functools.partial(front_kernel, outer, inner, cores, heads...  80.5 us
    unnamed x17, local copies, waits for them, and re-layouts  7.01 us

profile of v5, /device:TPU:0, one launch (start us, length us, event | category | flops | bytes accessed | tf_op | source)
XLA Modules:
  0.0 229.9 jit_solution(3141448049804300541)
XLA Ops:
  0.0 0.0 copy-start
  0.0 0.0 copy-start.2
  0.0 0.0 copy-start.1
  0.0 1.0 fusion.11.piece_ref
  1.0 0.9 copy.29
  1.9 0.6 fusion.8
  2.5 1.0 fusion
  3.5 1.0 fusion.2
  4.6 0.1 pad.12.clone
  4.6 0.1 maximum_maximum_fusion.row_ref
  4.7 0.2 multiply_sine_fusion.1
  4.9 1.5 copy.35
  6.4 1.2 copy.31.rope_ref
  7.7 0.0 copy-done
  7.7 0.0 copy-done.2
  7.7 0.0 copy-done.1
  7.7 0.0 copy-start.5
  7.7 0.0 copy-start.6
  7.8 80.5 %shard_map.145 = (f32[8,256,256]{2,1,0:T(8,128)S(1)}, bf16[8,256,256]{2,1,0:T(8,128)(2,1)S(1)}) custom-call(bf16[256,384]{1,0:T(8,128)(2,1)S(1)} %maximum_maximum_fusion.row_ref, bf16[128,512]{1,0:T(8,128)(2,1)S(1)} %fusion.11.piece_ref, bf16[256,512]{1,0:T(8,128)(2,1)S(1)} %copy-done.1, bf16[256,2048]{1,0:T(8,128)(2,1)S(1)} %bitcast.20, ...), custom_call_target="tpu_custom_call" | custom-call | flops 20000000000 | bytes 10000000 | tf_op jit(solution)/shard_map/pallas_call | solution.py:407
  88.2 0.0 copy-start.3
  88.2 1.3 copy-done.3
  89.6 0.0 copy-start.4
  89.6 1.0 copy-done.4
  90.5 0.0 copy-done.5
  90.6 0.6 reduce-window.6
  91.1 0.2 slice_reduce_fusion
  91.4 0.1 add_add_fusion
  91.5 0.0 copy-done.6
  91.6 0.6 select_maximum_fusion.meta_ref
  92.2 135.3 %shard_map.146 = bf16[256,2048]{1,0:T(8,128)(2,1)} custom-call(bf16[8,256,256]{2,1,0:T(8,128)(2,1)} %copy-done.4, f32[4,8,256]{2,1,0:T(8,128)} %select_maximum_fusion.meta_ref, f32[8,256,256]{2,1,0:T(8,128)} %copy-done.3, bf16[1,2048,1024]{2,1,0:T(8,128)(2,1)} %gate_hbm.1, bf16[1,2048,1024]{2,1,0:T(8,128)(2,1)} %up_hbm.1, bf16[1,1024,2048]{2,1,0:T(8,128)(2,1)} %down_hbm.1), custom_call_target="tpu_custom_call" | custom-call | flops 12884901888 | bytes 10000000 | tf_op jit(solution)/shard_map/pallas_call | solution.py:845
  227.5 2.3 %copy.37 = bf16[1,256,2048]{2,1,0:T(8,128)(2,1)} copy(bf16[1,256,2048]{2,1,0:T(8,128)(2,1)} %bitcast.24) | data formatting | bytes 2097152
  (15 shorter events, 0.2 us)
Async XLA Ops:
  0.0 7.7 %copy-start = (bf16[1,256,2048]{2,1,0:T(8,128)(2,1)S(1)}, bf16[1,256,2048]{2,1,0:T(8,128)(2,1)}, u32[]{:S(2)}) copy-start(bf16[1,256,2048]{2,1,0:T(8,128)(2,1)} %param.19) | copy-start | bytes 3145732
  0.0 7.7 %copy-start.2 = (f32[2048]{0:T(1024)S(1)}, f32[2048]{0:T(1024)}, u32[]{:S(2)}) copy-start(f32[2048]{0:T(1024)} %param.24) | copy-start | bytes 24580
  0.0 7.7 %copy-start.1 = (bf16[256,512]{1,0:T(8,128)(2,1)S(1)}, bf16[256,512]{1,0:T(8,128)(2,1)}, u32[]{:S(2)}) copy-start(bf16[256,512]{1,0:T(8,128)(2,1)} %block_ref.1) | copy-start | bytes 786436
  7.7 82.8 %copy-start.5 = (s32[1,256,2]{1,2,0:T(2,128)S(1)}, s32[1,256,2]{1,2,0:T(2,128)}, u32[]{:S(2)}) copy-start(s32[1,256,2]{1,2,0:T(2,128)} %param.28) | copy-start | bytes 6148
  7.7 83.8 %copy-start.6 = (f32[1,256,2]{1,2,0:T(2,128)S(1)}, f32[1,256,2]{1,2,0:T(2,128)}, u32[]{:S(2)}) copy-start(f32[1,256,2]{1,2,0:T(2,128)} %param.29) | copy-start | bytes 6148
  88.2 1.4 copy-start.3
  89.6 1.0 copy-start.4

commit v6 on v5

--- a/solution.py
+++ b/solution.py
@@ -13,6 +13,7 @@
 masked_score = -1e30
 log2_e = 1.4426950408889634
 part_width = 256
+extra_vmem = 3 * 2**19
 link_rate = 46.6e3
 link_delay = 2.2
 
@@ -47,7 +48,7 @@
 def front_kernel(
     outer, inner, cores, heads_here, nope, channels, scale,
     row_ref, piece_ref, block_ref, nope_ref, rope_ref, cosine_ref, sine_ref, resid_ref, gain_ref,
-    after_ref, normed_ref, shared, ups, weights, heads, queries, *sems,
+    routes_ref, route_weight_ref, after_ref, normed_ref, meta_ref, shared, ups, weights, heads, queries, *sems,
 ):
     me, dp = lax.axis_index("sp"), lax.axis_index("dp")
     z, y = me // inner, lax.rem(me, inner)
@@ -255,6 +256,25 @@
                 nope_ref[:, head * nope : (head + 1) * nope].astype(jnp.float32)
             ).astype(queries.dtype)
 
+    experts = meta_ref.shape[0] * inner
+    ids = lax.broadcasted_iota(jnp.int32, (experts, tokens), 0)
+    mine = [routes_ref[at : at + 1, :] == ids for at in range(routes_ref.shape[0])]
+    named = functools.reduce(jnp.logical_or, mine)
+    weight = sum(
+        jnp.where(chosen, route_weight_ref[at : at + 1, :], 0.0) for at, chosen in enumerate(mine)
+    )
+    earlier = lax.broadcasted_iota(jnp.int32, (tokens, tokens), 0)
+    upto = jnp.where(earlier < lax.broadcasted_iota(jnp.int32, (tokens, tokens), 1), 1.0, 0.0)
+    place = jnp.dot(
+        jnp.where(named, 1.0, 0.0).astype(jnp.bfloat16), upto.astype(jnp.bfloat16),
+        preferred_element_type=jnp.float32,
+    )
+    slot = jnp.where(named, place, -1.0)
+    meta_ref[...] = jnp.zeros_like(meta_ref)
+    for at in range(meta_ref.shape[0]):
+        meta_ref[at, 0:inner] = slot[at * inner : (at + 1) * inner]
+        meta_ref[at, inner : 2 * inner] = weight[at * inner : (at + 1) * inner]
+
     for turn in range(1, outer):
         row.from_z(turn)
         piece.from_z(turn)
@@ -266,9 +286,12 @@
         piece.from_y(index)
     piece.settle()
 
-    key_ids = lax.broadcasted_iota(jnp.int32, (tokens, tokens), 0)
-    query_ids = lax.broadcasted_iota(jnp.int32, (tokens, tokens), 1)
-    allowed = key_ids <= query_ids
+    span = 2 * tokens if groups % 2 == 0 else tokens
+    chunks = span // tokens
+    ending = me // chunks
+    key_ids = lax.broadcasted_iota(jnp.int32, (span, tokens), 0)
+    query_ids = lax.broadcasted_iota(jnp.int32, (span, tokens), 1)
+    allowed = key_ids <= query_ids + lax.rem(me, chunks) * tokens
 
     def attend_group(group):
         up = ups[:, group].reshape(channels, 2 * columns)
@@ -276,9 +299,10 @@
         up_values = up[:, columns : 2 * columns]
         up_values_t = jnp.transpose(up_values.astype(jnp.float32)).astype(jnp.bfloat16)
 
-        def scores_of(chunk):
-            latent = shared[chunk, :, 0:channels]
-            turned = shared[chunk, :, channels:]
+        def scores_of(place):
+            taken = shared[pl.ds(place * chunks, chunks)].reshape(span, shared.shape[2])
+            latent = taken[:, 0:channels]
+            turned = taken[:, channels:]
             keys = jnp.dot(latent, up_keys, preferred_element_type=jnp.float32).astype(jnp.bfloat16)
             values_t = lax.dot_general(
                 up_values_t, latent, (((1,), (1,)), ((), ())), preferred_element_type=jnp.float32
@@ -294,7 +318,7 @@
                 )
             return scores, [values_t[h * nope : (h + 1) * nope, :] for h in range(heads_here)]
 
-        scores, values = scores_of(me)
+        scores, values = scores_of(ending)
         state = []
         for score, value in zip(scores, values):
             score = jnp.where(allowed, score, masked_score)
@@ -308,8 +332,8 @@
                 )
             )
 
-        def step(chunk, state):
-            scores, values = scores_of(chunk)
+        def step(place, state):
+            scores, values = scores_of(place)
             after = []
             for (largest, total, kept), score, value in zip(state, scores, values):
                 now = jnp.maximum(largest, jnp.max(score, axis=0, keepdims=True))
@@ -327,7 +351,7 @@
                 )
             return tuple(after)
 
-        state = lax.fori_loop(0, me, step, tuple(state))
+        state = lax.fori_loop(0, ending, step, tuple(state))
         for head, (_, total, kept) in enumerate(state):
             start = pl.multiple_of(group * columns + head * nope, nope)
             heads[:, pl.ds(start, nope)] = jnp.transpose(kept / total).astype(heads.dtype)
@@ -384,8 +408,8 @@
 
 
 def run_front(
-    row, piece, block, query_nope, query_rope, cosine, sine_part, resid, gain,
-    sp_count, dp_count, cores, heads_here, nope, channels, scale, number,
+    row, piece, block, query_nope, query_rope, cosine, sine_part, resid, gain, routes, route_weight,
+    experts, sp_count, dp_count, cores, heads_here, nope, channels, scale, number,
 ):
     outer, inner = split_of(sp_count)
     lanes = dp_count // cores
@@ -409,9 +433,12 @@
         out_shape=[
             jax.ShapeDtypeStruct((model // width, tokens, width), jnp.float32),
             jax.ShapeDtypeStruct((model // width, tokens, width), jnp.bfloat16),
+            jax.ShapeDtypeStruct(
+                (outer, 2 * experts // outer + -2 * experts // outer % 8, tokens), jnp.float32
+            ),
         ],
-        in_specs=[vmem] * 9,
-        out_specs=[vmem] * 2,
+        in_specs=[vmem] * 11,
+        out_specs=[vmem] * 3,
         scratch_shapes=[
             pltpu.VMEM((sp_count,) + row.shape, row.dtype),
             pltpu.VMEM((cores, sp_count) + piece.shape, piece.dtype),
@@ -429,7 +456,9 @@
             collective_id=number, has_side_effects=True, vmem_limit_bytes=40 * 2**20
         ),
         cost_estimate=pl.CostEstimate(flops=2 * 10**10, bytes_accessed=10**7, transcendentals=0),
-    )(row, piece, block, query_nope, query_rope, cosine, sine_part, resid, gain)
+    )(
+        row, piece, block, query_nope, query_rope, cosine, sine_part, resid, gain, routes, route_weight
+    )
 
 
 def split_of(sp_count):
@@ -842,29 +871,35 @@
     steps_y = max(inner - 1, 1)
     vmem = pl.BlockSpec(memory_space=pltpu.VMEM)
     anywhere = pl.BlockSpec(memory_space=pl.ANY)
+    held = [
+        pltpu.VMEM((model, hidden), bf16),
+        pltpu.VMEM((model, hidden), bf16),
+        pltpu.VMEM((hidden, model), bf16),
+        pltpu.VMEM((outer, parts, tokens, width), bf16),
+        pltpu.VMEM((outer,) + meta.shape[1:], f32),
+        pltpu.VMEM((outer, inner, parts, capacity, width), bf16),
+        pltpu.VMEM((outer, inner, parts, capacity, width), bf16),
+        pltpu.VMEM((outer, inner, parts, capacity, width), bf16),
+        pltpu.VMEM((outer, inner, parts, capacity, width), bf16),
+        pltpu.VMEM((outer, parts, tokens, width), bf16),
+        pltpu.VMEM((outer + 1, parts, tokens, width), bf16),
+        pltpu.VMEM((parts, tokens, width), f32),
+        pltpu.VMEM((inner * capacity, hidden), f32),
+        pltpu.VMEM((inner * capacity, hidden), f32),
+        pltpu.VMEM((outer, inner * capacity, tokens), bf16),
+        pltpu.VMEM((outer, tokens, meta.shape[1]), f32),
+        pltpu.VMEM((outer, inner, tokens, capacity), bf16),
+    ]
+    grant = sum(
+        math.prod(s.shape[:-1]) * -(-s.shape[-1] // 128) * 128 * s.dtype.itemsize for s in held
+    )
     return pl.pallas_call(
         functools.partial(experts_kernel, outer, inner, capacity, order),
         out_shape=jax.ShapeDtypeStruct((tokens, parts * width), bf16),
         in_specs=[vmem, vmem, vmem, anywhere, anywhere, anywhere],
         out_specs=vmem,
-        scratch_shapes=[
-            pltpu.VMEM((model, hidden), bf16),
-            pltpu.VMEM((model, hidden), bf16),
-            pltpu.VMEM((hidden, model), bf16),
-            pltpu.VMEM((outer, parts, tokens, width), bf16),
-            pltpu.VMEM((outer,) + meta.shape[1:], f32),
-            pltpu.VMEM((outer, inner, parts, capacity, width), bf16),
-            pltpu.VMEM((outer, inner, parts, capacity, width), bf16),
-            pltpu.VMEM((outer, inner, parts, capacity, width), bf16),
-            pltpu.VMEM((outer, inner, parts, capacity, width), bf16),
-            pltpu.VMEM((outer, parts, tokens, width), bf16),
-            pltpu.VMEM((outer + 1, parts, tokens, width), bf16),
-            pltpu.VMEM((parts, tokens, width), f32),
-            pltpu.VMEM((inner * capacity, hidden), f32),
-            pltpu.VMEM((inner * capacity, hidden), f32),
-            pltpu.VMEM((outer, inner * capacity, tokens), bf16),
-            pltpu.VMEM((outer, tokens, meta.shape[1]), f32),
-            pltpu.VMEM((outer, inner, tokens, capacity), bf16),
+        scratch_shapes=held
+        + [
             dma((3,)),
             dma((outer,)),
             dma((outer,)),
@@ -878,7 +913,7 @@
             dma((outer + 1, parts)),
         ],
         compiler_params=pltpu.CompilerParams(
-            collective_id=number, has_side_effects=True, vmem_limit_bytes=60 * 2**20
+            collective_id=number, has_side_effects=True, vmem_limit_bytes=grant + extra_vmem
         ),
         cost_estimate=pl.CostEstimate(
             flops=6 * sp_count * capacity * model * hidden, bytes_accessed=10**7, transcendentals=0
@@ -925,23 +960,13 @@
     )
     frequency = rope_base ** (-jnp.arange(rope // 2, dtype=jnp.float32) / (rope // 2))
     angles = frequency[:, None] * local_pos.astype(jnp.float32)[None, :]
-    after, normed = run_front(
-        row, ups, out_proj, query_nope[0].reshape(tokens, -1), query_rope[0].reshape(tokens, -1),
-        jnp.cos(angles), jnp.sin(angles), resid[0], norm_gain[None],
-        sp_count, dp_count, cores, heads_here, nope, channels, scale, 0,
-    )
-
     experts_all = sp_count * expert_gate.shape[0]
     capacity = 4 * tokens // experts_all
-    ids = jnp.arange(experts_all, dtype=jnp.int32)[:, None, None]
-    mine = routes[0][None] == ids
-    named = jnp.any(mine, axis=-1)
-    weight = jnp.sum(jnp.where(mine, route_weight[0][None], 0.0), axis=-1)
-    place = jnp.cumsum(named.astype(jnp.int32), axis=1) - 1
-    outer, inner = split_of(sp_count)
-    slot = jnp.where(named, place, -1).astype(jnp.float32).reshape(outer, inner, tokens)
-    meta = jnp.concatenate([slot, weight.reshape(outer, inner, tokens)], axis=1)
-    meta = jnp.pad(meta, ((0, 0), (0, -2 * inner % 8), (0, 0)))
+    after, normed, meta = run_front(
+        row, ups, out_proj, query_nope[0].reshape(tokens, -1), query_rope[0].reshape(tokens, -1),
+        jnp.cos(angles), jnp.sin(angles), resid[0], norm_gain[None], routes[0].T, route_weight[0].T,
+        experts_all, sp_count, dp_count, cores, heads_here, nope, channels, scale, 0,
+    )
     mixed = run_experts(
         normed, meta, after, expert_gate, expert_up, expert_down, sp_count, capacity, 1
     )

time: 230 us -> 216 us (0.939)
  Pallas kernels: 216 us -> 207 us
  local copies, waits for them, and re-layouts: 8.61 us -> 4.69 us
    pallas_call x1, Pallas kernels: 135 us -> 127 us  [run_experts(): pl.pallas_call(functools.partial(experts_kernel, outer, inner, capacity,...]
    unnamed x17 -> x13, local copies, waits for them, and re-layouts: 7.01 us -> 3.36 us
where the time goes in v6:
time: 216 us
  Pallas kernels  207 us (96%)
  local copies, waits for them, and re-layouts  4.69 us (2%)
  other arithmetic  3.92 us (2%)
    pallas_call x1, Pallas kernels, run_experts(): pl.pallas_call(functools.partial(experts_kernel, outer, inner, capacity,...  127 us
    pallas_call x1, Pallas kernels, run_front(): pl.pallas_call(functools.partial(front_kernel, outer, inner, cores, heads...  80.3 us

profile of v6, /device:TPU:0, one launch (start us, length us, event | category | flops | bytes accessed | tf_op | source)
XLA Modules:
  0.0 215.7 jit_solution(17403401617789425748)
XLA Ops:
  0.0 0.0 copy-start.4
  0.0 0.0 copy-start.3
  0.0 0.0 copy-start.2
  0.0 0.0 copy-start.1
  0.0 0.0 copy-start
  0.1 0.1 pad.5.clone
  0.1 1.1 fusion
  1.3 0.9 copy.20
  2.2 0.6 fusion.8
  2.8 0.2 multiply_sine_fusion.1
  3.0 1.0 fusion.2
  4.0 0.1 maximum_maximum_fusion.row_ref
  4.1 0.9 fusion.11.piece_ref
  5.0 1.2 copy.22.rope_ref
  6.2 1.5 copy.25
  7.7 0.0 copy-done.4
  7.7 0.0 copy-done.3
  7.7 0.0 copy-done.2
  7.8 0.0 copy-done.1
  7.8 0.0 copy-done
  7.8 80.3 %shard_map.145 = (f32[8,256,256]{2,1,0:T(8,128)S(1)}, bf16[8,256,256]{2,1,0:T(8,128)(2,1)S(1)}, f32[4,8,256]{2,1,0:T(8,128)S(1)}) custom-call(bf16[256,384]{1,0:T(8,128)(2,1)S(1)} %maximum_maximum_fusion.row_ref, bf16[128,512]{1,0:T(8,128)(2,1)S(1)} %fusion.11.piece_ref, bf16[256,512]{1,0:T(8,128)(2,1)S(1)} %copy-done.1, bf16[256,2048]{1,0:T(8,128)(2,1)S(1)} %bitcast.22, ...), custom_call_target="tpu_custom_call" | custom-call | flops 20000000000 | bytes 10000000 | tf_op jit(solution)/shard_map/pallas_call | solution.py:431
  88.1 126.7 %shard_map.146 = bf16[256,2048]{1,0:T(8,128)(2,1)S(1)} custom-call(bf16[8,256,256]{2,1,0:T(8,128)(2,1)S(1)} %get-tuple-element.8.normed_ref, f32[4,8,256]{2,1,0:T(8,128)S(1)} %get-tuple-element.9.meta_ref, f32[8,256,256]{2,1,0:T(8,128)S(1)} %get-tuple-element.10.after_ref, bf16[1,2048,1024]{2,1,0:T(8,128)(2,1)} %gate_hbm.1, bf16[1,2048,1024]{2,1,0:T(8,128)(2,1)} %up_hbm.1, ...), custom_call_target="tpu_custom_call" | custom-call | flops 12884901888 | bytes 10000000 | tf_op jit(solution)/shard_map/pallas_call | solution.py:896
  214.8 1.0 copy.27
  (5 shorter events, 0.0 us)
Async XLA Ops:
  0.0 7.7 %copy-start.4 = (f32[1,256,2]{1,2,0:T(2,128)S(1)}, f32[1,256,2]{1,2,0:T(2,128)}, u32[]{:S(2)}) copy-start(f32[1,256,2]{1,2,0:T(2,128)} %param.29) | copy-start | bytes 6148
  0.0 7.7 %copy-start.3 = (s32[1,256,2]{1,2,0:T(2,128)S(1)}, s32[1,256,2]{1,2,0:T(2,128)}, u32[]{:S(2)}) copy-start(s32[1,256,2]{1,2,0:T(2,128)} %param.28) | copy-start | bytes 6148
  0.0 7.7 %copy-start.2 = (f32[2048]{0:T(1024)S(1)}, f32[2048]{0:T(1024)}, u32[]{:S(2)}) copy-start(f32[2048]{0:T(1024)} %param.24) | copy-start | bytes 24580
  0.0 7.7 %copy-start.1 = (bf16[256,512]{1,0:T(8,128)(2,1)S(1)}, bf16[256,512]{1,0:T(8,128)(2,1)}, u32[]{:S(2)}) copy-start(bf16[256,512]{1,0:T(8,128)(2,1)} %block_ref.1) | copy-start | bytes 786436
  0.0 7.8 %copy-start = (bf16[1,256,2048]{2,1,0:T(8,128)(2,1)S(1)}, bf16[1,256,2048]{2,1,0:T(8,128)(2,1)}, u32[]{:S(2)}) copy-start(bf16[1,256,2048]{2,1,0:T(8,128)(2,1)} %param.19) | copy-start | bytes 3145732

commit v7 on v6

--- a/solution.py
+++ b/solution.py
@@ -171,11 +171,14 @@
             for step in range(1, cores):
                 self.across(step, 0, index).start()
 
-        def from_z(self, turn):
+        def reach_z(self, turn):
             self.wait(self.place(member(turn)), self.sems[1].at[source_of(turn)])
             self.start_z(turn)
+            self.start_wide(turn)
+
+        def from_z(self, turn):
+            self.reach_z(turn)
             self.start_y(turn)
-            self.start_wide(turn)
 
         def from_y(self, index):
             step = inner - index // outer
@@ -233,6 +236,7 @@
         spread.start_y(0)
         spread.start_wide(0)
     block.start_z(0)
+    block.start_y(0)
     block.start_wide(0)
     shared[me] = row_ref[...]
     ups[core, me] = piece_ref[...]
@@ -275,11 +279,15 @@
         meta_ref[at, 0:inner] = slot[at * inner : (at + 1) * inner]
         meta_ref[at, inner : 2 * inner] = weight[at * inner : (at + 1) * inner]
 
-    for turn in range(1, outer):
+    for turn in range(1, outer - 1):
         row.from_z(turn)
         piece.from_z(turn)
-    block.start_y(0)
-    for turn in range(1, outer - 1):
+    block.reach_z(1)
+    block.from_y(outer)
+    row.from_z(outer - 1)
+    piece.from_z(outer - 1)
+    block.start_y(1)
+    for turn in range(2, outer - 1):
         block.from_z(turn)
     for index in range(outer, groups):
         row.from_y(index)
@@ -363,7 +371,7 @@
         def _():
             block.from_z(outer - 1)
 
-        nearby = group + outer - 1
+        nearby = group + outer
 
         @pl.when((group > 0) & (nearby < groups))
         def _():

time: 216 us -> 216 us (level)
  no operation moved by 1% of the time
where the time goes in v7:
time: 216 us
  Pallas kernels  207 us (96%)
  local copies, waits for them, and re-layouts  4.69 us (2%)
  other arithmetic  3.92 us (2%)
    pallas_call x1, Pallas kernels, run_experts(): pl.pallas_call(functools.partial(experts_kernel, outer, inner, capacity,...  127 us
    pallas_call x1, Pallas kernels, run_front(): pl.pallas_call(functools.partial(front_kernel, outer, inner, cores, heads...  79.9 us

profile of v7, /device:TPU:0, one launch (start us, length us, event | category | flops | bytes accessed | tf_op | source)
XLA Modules:
  0.0 215.7 jit_solution(1619647798917102707)
XLA Ops:
  0.0 0.0 copy-start.4
  0.0 0.0 copy-start.3
  0.0 0.0 copy-start.2
  0.0 0.0 copy-start.1
  0.0 0.0 copy-start
  0.1 0.1 pad.5.clone
  0.1 1.1 fusion
  1.3 0.9 copy.20
  2.2 0.6 fusion.8
  2.8 0.2 multiply_sine_fusion.1
  3.0 1.0 fusion.2
  4.0 0.1 maximum_maximum_fusion.row_ref
  4.1 0.9 fusion.11.piece_ref
  5.0 1.2 copy.22.rope_ref
  6.2 1.5 copy.25
  7.7 0.0 copy-done.4
  7.7 0.0 copy-done.3
  7.7 0.0 copy-done.2
  7.8 0.0 copy-done.1
  7.8 0.0 copy-done
  7.8 79.9 %shard_map.145 = (f32[8,256,256]{2,1,0:T(8,128)S(1)}, bf16[8,256,256]{2,1,0:T(8,128)(2,1)S(1)}, f32[4,8,256]{2,1,0:T(8,128)S(1)}) custom-call(bf16[256,384]{1,0:T(8,128)(2,1)S(1)} %maximum_maximum_fusion.row_ref, bf16[128,512]{1,0:T(8,128)(2,1)S(1)} %fusion.11.piece_ref, bf16[256,512]{1,0:T(8,128)(2,1)S(1)} %copy-done.1, bf16[256,2048]{1,0:T(8,128)(2,1)S(1)} %bitcast.22, ...), custom_call_target="tpu_custom_call" | custom-call | flops 20000000000 | bytes 10000000 | tf_op jit(solution)/shard_map/pallas_call | solution.py:439
  87.7 126.9 %shard_map.146 = bf16[256,2048]{1,0:T(8,128)(2,1)S(1)} custom-call(bf16[8,256,256]{2,1,0:T(8,128)(2,1)S(1)} %get-tuple-element.8.normed_ref, f32[4,8,256]{2,1,0:T(8,128)S(1)} %get-tuple-element.9.meta_ref, f32[8,256,256]{2,1,0:T(8,128)S(1)} %get-tuple-element.10.after_ref, bf16[1,2048,1024]{2,1,0:T(8,128)(2,1)} %gate_hbm.1, bf16[1,2048,1024]{2,1,0:T(8,128)(2,1)} %up_hbm.1, ...), custom_call_target="tpu_custom_call" | custom-call | flops 12884901888 | bytes 10000000 | tf_op jit(solution)/shard_map/pallas_call | solution.py:904
  214.7 1.0 copy.27
  (5 shorter events, 0.0 us)
Async XLA Ops:
  0.0 7.7 %copy-start.4 = (f32[1,256,2]{1,2,0:T(2,128)S(1)}, f32[1,256,2]{1,2,0:T(2,128)}, u32[]{:S(2)}) copy-start(f32[1,256,2]{1,2,0:T(2,128)} %param.29) | copy-start | bytes 6148
  0.0 7.7 %copy-start.3 = (s32[1,256,2]{1,2,0:T(2,128)S(1)}, s32[1,256,2]{1,2,0:T(2,128)}, u32[]{:S(2)}) copy-start(s32[1,256,2]{1,2,0:T(2,128)} %param.28) | copy-start | bytes 6148
  0.0 7.7 %copy-start.2 = (f32[2048]{0:T(1024)S(1)}, f32[2048]{0:T(1024)}, u32[]{:S(2)}) copy-start(f32[2048]{0:T(1024)} %param.24) | copy-start | bytes 24580
  0.0 7.7 %copy-start.1 = (bf16[256,512]{1,0:T(8,128)(2,1)S(1)}, bf16[256,512]{1,0:T(8,128)(2,1)}, u32[]{:S(2)}) copy-start(bf16[256,512]{1,0:T(8,128)(2,1)} %block_ref.1) | copy-start | bytes 786436
  0.0 7.8 %copy-start = (bf16[1,256,2048]{2,1,0:T(8,128)(2,1)S(1)}, bf16[1,256,2048]{2,1,0:T(8,128)(2,1)}, u32[]{:S(2)}) copy-start(bf16[1,256,2048]{2,1,0:T(8,128)(2,1)} %param.19) | copy-start | bytes 3145732
